TPU v7x, 32 devices: a whole 2x2x4 slice. The times are simulated.
32 devices in a mesh: dp: 4 (over y, x), kv: 4 (over z), tp: 2 (over core).
Axes of the slice: x: 2, y: 2, z: 4, core: 2. Of those that a mesh axis runs over, the one named last changes fastest.
Arguments:
- tokens: bfloat16 [64, 2048], P('dp', ('kv', 'tp')), may hold values from -30 to 30
- state: float32 [64, 4, 256, 512], P(('dp', 'kv'), 'tp'), may hold values from -6 to 6
- mix_gain: float32 [2048], P('kv'), may hold values from 0.1 to 1.9
- w_query: bfloat16 [2048, 1024], P('kv', 'tp'), may hold values from -0.125 to 0.125
- w_key: bfloat16 [2048, 1024], P('kv', 'tp'), may hold values from -0.125 to 0.125
- w_decay: bfloat16 [2048, 1024], P('kv', 'tp'), may hold values from -0.125 to 0.125
- w_value: bfloat16 [2048, 2048], P('kv', 'tp'), may hold values from -0.125 to 0.125
- w_gate: bfloat16 [2048, 2048], P('kv', 'tp'), may hold values from -0.125 to 0.125
- decay_offset: float32 [1024], P('tp'), may hold values from -1 to 4
- head_gain: float32 [512], replicated, may hold values from 0.1 to 1.9
- w_out: bfloat16 [2048, 2048], P('tp', 'kv'), may hold values from -0.125 to 0.125
- mlp_gain: float32 [2048], replicated, may hold values from 0.1 to 1.9
- w_up: bfloat16 [2048, 8192], P(None, ('kv', 'tp')), may hold values from -0.125 to 0.125
- w_down: bfloat16 [8192, 2048], P(('kv', 'tp')), may hold values from -0.09375 to 0.09375
Outputs:
- mixed: bfloat16 [64, 2048], P('dp', ('kv', 'tp'))
- new_state: float32 [64, 4, 256, 512], P(('dp', 'kv'), 'tp')
All inputs are finite; a program needn't handle non-finite values.
Results may differ from a plain program's by a relative error of at most 0.013.
Values may be sent and summed in bfloat16 or wider, within the bound.
A program may use at most 64 MiB of HBM per device.

v0:
```python
import functools

import jax
import jax.numpy as jnp
from jax import lax
from jax.experimental import pallas as pl
from jax.experimental.pallas import tpu as pltpu
from jax.sharding import PartitionSpec as P

D = 2048


epsilon = 1e-06


def plain_shards(
    tokens,
    state,
    mix_gain,
    w_query,
    w_key,
    w_decay,
    w_value,
    w_gate,
    decay_offset,
    head_gain,
    w_out,
    mlp_gain,
    w_up,
    w_down,
):
    seq_dev = state.shape[0]
    heads_here = state.shape[1]
    key_dim = state.shape[2]
    val_dim = state.shape[3]
    weights = (w_query, w_key, w_decay, w_value, w_gate)
    tok_cols = lax.all_gather(tokens, "tp", axis=1, tiled=True)
    tok_float = tok_cols.astype(jnp.float32)
    squares = jnp.sum(tok_float * tok_float, axis=1)
    scaled = (tok_float * mix_gain).astype(jnp.bfloat16)
    kv_index = lax.axis_index("kv")
    projected = lax.psum_scatter(
        jnp.concatenate(
            [jnp.dot(scaled, weight, preferred_element_type=jnp.float32) for weight in weights],
            axis=1,
        ),
        "kv",
        scatter_dimension=0,
        tiled=True,
    )
    all_sums = lax.psum(squares, "kv")
    row_sums = lax.dynamic_slice_in_dim(all_sums, kv_index * seq_dev, seq_dev, 0)
    row_scale = lax.rsqrt(row_sums / D + epsilon)[:, None]
    projected = projected * row_scale
    key_width = heads_here * key_dim
    val_width = heads_here * val_dim
    queries = (projected[:, :key_width] * key_dim ** (-0.5)).reshape(seq_dev, heads_here, key_dim)
    new_keys = projected[:, key_width : 2 * key_width].reshape(seq_dev, heads_here, key_dim)
    retain = jax.nn.sigmoid(projected[:, 2 * key_width : 3 * key_width] + decay_offset).reshape(
        seq_dev, heads_here, key_dim
    )
    values = projected[:, 3 * key_width : 3 * key_width + val_width].reshape(
        seq_dev, heads_here, val_dim
    )
    gates = projected[:, 3 * key_width + val_width :]
    new_state = retain[..., None] * state + new_keys[..., None] * values[:, :, None, :]
    readout = jnp.einsum("bhk,bhkv->bhv", queries, new_state, precision=lax.Precision.HIGHEST)
    readout = (
        readout
        * lax.rsqrt(jnp.mean(readout * readout, axis=2, keepdims=True) + epsilon)
        * head_gain
    )
    gated = (readout.reshape(seq_dev, val_width) * jax.nn.silu(gates)).astype(jnp.bfloat16)
    branch = jnp.dot(
        lax.all_gather(gated, "kv", axis=0, tiled=True), w_out, preferred_element_type=jnp.float32
    )
    own_width = tokens.shape[1]
    branch_total = lax.psum(branch.astype(jnp.bfloat16), "tp").astype(jnp.float32)
    stream_cols = (tok_float + branch_total).astype(jnp.bfloat16)
    stream = lax.all_gather(stream_cols, "kv", axis=1, tiled=True)
    stream_own = lax.dynamic_slice_in_dim(
        stream_cols, lax.axis_index("tp") * own_width, own_width, 1
    )
    stream_float = stream.astype(jnp.float32)
    mlp_scale = lax.rsqrt(jnp.mean(stream_float * stream_float, axis=1, keepdims=True) + epsilon)
    normed = (stream_float * mlp_gain).astype(jnp.bfloat16)
    hidden = jnp.dot(normed, w_up, preferred_element_type=jnp.float32) * mlp_scale
    squared = jnp.square(jax.nn.relu(hidden)).astype(jnp.bfloat16)
    down_own = lax.psum_scatter(
        lax.dot_general(
            w_down, squared, (((0,), (1,)), ((), ())), preferred_element_type=jnp.float32
        ),
        ("kv", "tp"),
        scatter_dimension=0,
        tiled=True,
    )
    mixed = (stream_own.astype(jnp.float32) + down_own.T).astype(jnp.bfloat16)
    return (mixed, new_state)


MESH = pl.DeviceIdType.MESH
ROW_CHUNK = 64
VMEM_BYTES = 67_043_328


def layer_kernel(
    n_kv,
    tok_hbm,
    mix_gain_hbm,
    decay_offset_hbm,
    head_gain_hbm,
    mlp_gain_hbm,
    state_hbm,
    wq_hbm,
    wk_hbm,
    wd_hbm,
    wv_hbm,
    wg_hbm,
    w_out_hbm,
    w_up_hbm,
    w_down_hbm,
    mixed_ref,
    state_ref,
    tok_ref,
    mix_gain_ref,
    decay_offset_ref,
    head_gain_ref,
    mlp_gain_ref,
    wq_ref,
    wk_ref,
    wd_ref,
    wv_ref,
    wg_ref,
    w_out_ref,
    w_up_ref,
    w_down_ref,
    tok_all,
    send_a,
    send_b,
    send_c,
    recv_a,
    recv_b,
    recv_c,
    coef,
    coef_t,
    vals,
    read,
    gated_all,
    gated_rows,
    branch_own,
    branch_other,
    stream_all,
    down_send,
    down_recv,
    load_sem,
    tok_sem,
    proj_send_sem,
    proj_recv_sem,
    gated_send_sem,
    gated_recv_sem,
    branch_sem,
    stream_send_sem,
    stream_recv_sem,
    down_send_sem,
    down_recv_sem,
):
    f32, bf16 = jnp.float32, jnp.bfloat16
    kv, tp = lax.axis_index("kv"), lax.axis_index("tp")
    other = 1 - tp
    rows, half = tok_ref.shape
    seqs, heads, key_dim, val_dim = state_ref.shape
    key_width, val_width = heads * key_dim, heads * val_dim
    width = 2 * n_kv * half

    def peer(offset):
        return lax.rem(kv + offset, n_kv)

    barrier = pltpu.get_barrier_semaphore()
    for offset in range(n_kv):
        for to_tp in (tp, other):
            if offset == 0 and to_tp is tp:
                continue
            pl.semaphore_signal(
                barrier, inc=1, device_id={"kv": peer(offset), "tp": to_tp}, device_id_type=MESH
            )

    loads = {}
    for at, (name, source, target) in enumerate(
        (
            ("tokens", tok_hbm, tok_ref),
            ("mix_gain", mix_gain_hbm, mix_gain_ref),
            ("q", wq_hbm, wq_ref),
            ("k", wk_hbm, wk_ref),
            ("d", wd_hbm, wd_ref),
            ("v", wv_hbm, wv_ref),
            ("g", wg_hbm, wg_ref),
            ("offset", decay_offset_hbm, decay_offset_ref),
            ("head_gain", head_gain_hbm, head_gain_ref),
            ("mlp_gain", mlp_gain_hbm, mlp_gain_ref),
            ("state", state_hbm, state_ref),
            ("out", w_out_hbm, w_out_ref),
            ("up", w_up_hbm, w_up_ref),
            ("down", w_down_hbm, w_down_ref),
        )
    ):
        loads[name] = pltpu.make_async_copy(source, target, load_sem.at[at])
        loads[name].start()
    loads["tokens"].wait()
    pl.semaphore_wait(barrier, 2 * n_kv - 1)

    tok_copy = pltpu.make_async_remote_copy(
        src_ref=tok_ref,
        dst_ref=tok_all.at[tp],
        send_sem=tok_sem.at[0],
        recv_sem=tok_sem.at[1],
        device_id={"kv": kv, "tp": other},
        device_id_type=MESH,
    )
    tok_copy.start()
    tok_own = tok_ref[...].astype(f32)
    squares = jnp.sum(tok_own * tok_own, axis=1, keepdims=True)
    for name in ("mix_gain", "offset", "head_gain", "mlp_gain"):
        loads[name].wait()
    tok_copy.wait_recv()
    tok_all[tp] = tok_ref[...]
    tok_other = tok_all[other].astype(f32)
    squares = squares + jnp.sum(tok_other * tok_other, axis=1, keepdims=True)
    scaled = jnp.concatenate(
        [(tok_all[i].astype(f32) * mix_gain_ref[i]).astype(bf16) for i in range(2)], axis=1
    )

    def project(name, weight_ref, send, at):
        loads[name].wait()
        total = jnp.dot(scaled, weight_ref[...], preferred_element_type=f32)
        columns = total.shape[1]
        for owner in range(n_kv):
            send[owner, :, at : at + columns] = total[owner * seqs : (owner + 1) * seqs].astype(bf16)

    def send_group(group, send, recv):
        copies = []
        for offset in reversed(range(1, n_kv)):
            copy = pltpu.make_async_remote_copy(
                src_ref=send.at[peer(offset)],
                dst_ref=recv.at[offset - 1],
                send_sem=proj_send_sem.at[group, offset - 1],
                recv_sem=proj_recv_sem.at[group, offset - 1],
                device_id={"kv": peer(offset), "tp": tp},
                device_id_type=MESH,
            )
            copy.start()
            copies.append(copy)
        return copies

    wide = jnp.broadcast_to(squares, (rows, 128))
    lane = lax.broadcasted_iota(jnp.int32, (seqs, 128), 1)
    for owner in range(n_kv):
        mine = slice(owner * seqs, (owner + 1) * seqs)
        high = wide[mine].astype(bf16).astype(f32)
        sums = jnp.where(lane < 64, high, wide[mine] - high)
        send_a[owner, :, 3 * key_width :] = sums.astype(bf16)
    project("q", wq_ref, send_a, 0)
    project("k", wk_ref, send_a, key_width)
    project("d", wd_ref, send_a, 2 * key_width)
    copies_a = send_group(0, send_a, recv_a)
    project("v", wv_ref, send_b, 0)
    copies_b = send_group(1, send_b, recv_b)
    project("g", wg_ref, send_c, 0)
    copies_c = send_group(2, send_c, recv_c)

    def gathered(copies, send, recv):
        total = send[kv].astype(f32)
        for copy in copies:
            copy.wait_recv()
        for offset in range(n_kv - 1):
            total = total + recv[offset].astype(f32)
        return total

    group_a = gathered(copies_a, send_a, recv_a)
    row_sums = group_a[:, 3 * key_width : 3 * key_width + 1] + group_a[:, 3 * key_width + 64 : 3 * key_width + 65]
    row_scale = lax.rsqrt(row_sums * (1.0 / width) + epsilon)
    queries = group_a[:, :key_width] * (row_scale * key_dim**-0.5)
    new_keys = group_a[:, key_width : 2 * key_width] * row_scale
    retain = jax.nn.sigmoid(
        group_a[:, 2 * key_width : 3 * key_width] * row_scale + decay_offset_ref[...]
    )
    query_retain = queries * retain
    overlap = queries * new_keys
    for h in range(heads):
        cols = slice(h * key_dim, (h + 1) * key_dim)
        coef[(3 * h) * seqs : (3 * h + 1) * seqs, :] = query_retain[:, cols]
        coef[(3 * h + 1) * seqs : (3 * h + 2) * seqs, :] = new_keys[:, cols]
        coef[(3 * h + 2) * seqs : (3 * h + 3) * seqs, :] = retain[:, cols]
    coef_t[...] = coef[...].T
    loads["state"].wait()
    for h in range(heads):
        for b in range(seqs):
            at = 3 * h * seqs + b
            total = jnp.zeros((8, val_dim), f32)
            for start in range(0, key_dim, ROW_CHUNK):
                piece = slice(start, start + ROW_CHUNK)
                product = coef_t[piece, at : at + 1] * state_ref[b, h, piece, :]
                total = total + jnp.sum(product.reshape(ROW_CHUNK // 8, 8, val_dim), axis=0)
            read[h, b : b + 1, :] = jnp.sum(total, axis=0, keepdims=True)

    values = gathered(copies_b, send_b, recv_b) * row_scale
    vals[...] = values
    gates = gathered(copies_c, send_c, recv_c) * row_scale
    for h in range(heads):
        cols = slice(h * val_dim, (h + 1) * val_dim)
        dots = jnp.sum(overlap[:, h * key_dim : (h + 1) * key_dim], axis=1, keepdims=True)
        readout = read[h] + dots * values[:, cols]
        mean = jnp.mean(readout * readout, axis=1, keepdims=True)
        gate = gates[:, cols]
        gated_all[kv, :, cols] = (
            readout * lax.rsqrt(mean + epsilon) * head_gain_ref[...] * (gate * jax.nn.sigmoid(gate))
        ).astype(bf16)

    gated_copies = []
    for offset in range(1, n_kv):
        copy = pltpu.make_async_remote_copy(
            src_ref=gated_all.at[kv],
            dst_ref=gated_all.at[kv],
            send_sem=gated_send_sem.at[offset - 1],
            recv_sem=gated_recv_sem.at[offset - 1],
            device_id={"kv": peer(offset), "tp": tp},
            device_id_type=MESH,
        )
        copy.start()
        gated_copies.append(copy)

    for h in range(heads):
        for b in range(seqs):
            at = 3 * h * seqs + b
            value_row = vals[b : b + 1, h * val_dim : (h + 1) * val_dim]
            for start in range(0, key_dim, ROW_CHUNK):
                piece = slice(start, start + ROW_CHUNK)
                state_ref[b, h, piece, :] = (
                    coef_t[piece, at + 2 * seqs : at + 2 * seqs + 1] * state_ref[b, h, piece, :]
                    + coef_t[piece, at + seqs : at + seqs + 1] * value_row
                )

    for copy in gated_copies:
        copy.wait_recv()
    for owner in range(n_kv):
        gated_rows[owner * seqs : (owner + 1) * seqs, :] = gated_all[owner].astype(f32)
    loads["out"].wait()
    branch = jnp.dot(gated_rows[...].astype(bf16), w_out_ref[...], preferred_element_type=f32)
    for i in range(2):
        branch_own[i] = branch[:, i * half : (i + 1) * half]
    branch_copy = pltpu.make_async_remote_copy(
        src_ref=branch_own,
        dst_ref=branch_other,
        send_sem=branch_sem.at[0],
        recv_sem=branch_sem.at[1],
        device_id={"kv": kv, "tp": other},
        device_id_type=MESH,
    )
    branch_copy.start()
    branch_copy.wait_recv()
    for i in range(2):
        stream_all[kv, i] = (tok_all[i].astype(f32) + (branch_own[i] + branch_other[i])).astype(bf16)
    stream_copies = []
    for offset in range(1, n_kv):
        copy = pltpu.make_async_remote_copy(
            src_ref=stream_all.at[kv],
            dst_ref=stream_all.at[kv],
            send_sem=stream_send_sem.at[offset - 1],
            recv_sem=stream_recv_sem.at[offset - 1],
            device_id={"kv": peer(offset), "tp": tp},
            device_id_type=MESH,
        )
        copy.start()
        stream_copies.append(copy)

    loads["up"].wait()
    hidden = None
    sums = None
    for step in UP_ORDER(n_kv):
        if step > 0:
            stream_copies[step - 1].wait_recv()
        owner = lax.rem(kv + n_kv - step, n_kv)
        pieces = [stream_all[owner, i].astype(f32) for i in range(2)]
        normed = jnp.concatenate(
            [(piece * mlp_gain_ref[owner, i]).astype(bf16) for i, piece in enumerate(pieces)], axis=1
        )
        first = pl.multiple_of(owner * (2 * half), 2 * half)
        term = jnp.dot(normed, w_up_ref[pl.ds(first, 2 * half), :], preferred_element_type=f32)
        part = sum(jnp.sum(piece * piece, axis=1, keepdims=True) for piece in pieces)
        hidden = term if hidden is None else hidden + term
        sums = part if sums is None else sums + part
    mlp_scale = lax.rsqrt(sums * (1.0 / width) + epsilon)
    active = jnp.maximum(hidden * mlp_scale, 0.0)
    squared = (active * active).astype(bf16)

    loads["down"].wait()

    def down_columns(offset, to_tp):
        block = peer(offset) * 2 + to_tp
        first = pl.multiple_of(block * half, half)
        return jnp.dot(squared, w_down_ref[:, pl.ds(first, half)], preferred_element_type=f32)

    down_copies = []
    for offset in UP_ORDER(n_kv)[::-1]:
        for flip in (1, 0):
            if offset == 0 and flip == 0:
                continue
            to_tp = other if flip else tp
            slot = offset * 2 + flip - 1
            down_send[slot] = down_columns(offset, to_tp).astype(bf16)
            copy = pltpu.make_async_remote_copy(
                src_ref=down_send.at[slot],
                dst_ref=down_recv.at[slot],
                send_sem=down_send_sem.at[slot],
                recv_sem=down_recv_sem.at[slot],
                device_id={"kv": peer(offset), "tp": to_tp},
                device_id_type=MESH,
            )
            copy.start()
            down_copies.append((slot, copy))
    total = stream_all[kv, tp].astype(f32) + down_columns(0, tp)
    for slot, copy in down_copies:
        copy.wait_recv()
        total = total + down_recv[slot].astype(f32)
    mixed_ref[...] = total.astype(bf16)

    tok_copy.wait_send()
    branch_copy.wait_send()
    for copy in copies_a + copies_b + copies_c + gated_copies + stream_copies:
        copy.wait_send()
    for _, copy in down_copies:
        copy.wait_send()


def write_kernel(mixed_ref, state_ref, mixed_hbm, state_hbm, state_sem, mixed_sem):
    seqs, heads = state_ref.shape[:2]
    copies = [pltpu.make_async_copy(mixed_ref, mixed_hbm, mixed_sem.at[0])]
    for b in range(seqs):
        for h in range(heads):
            copies.append(
                pltpu.make_async_copy(state_ref.at[b, h], state_hbm.at[b, h], state_sem.at[b, h])
            )
    for copy in copies:
        copy.start()
    for copy in copies:
        copy.wait()


def UP_ORDER(n_kv):
    return sorted(range(n_kv), key=lambda offset: min(offset, n_kv - offset))


def kernel_shards(
    n_kv,
    tokens,
    state,
    mix_gain,
    w_query,
    w_key,
    w_decay,
    w_value,
    w_gate,
    decay_offset,
    head_gain,
    w_out,
    mlp_gain,
    w_up,
    w_down,
):
    f32, bf16 = jnp.float32, jnp.bfloat16
    rows, half = tokens.shape
    seqs, heads, key_dim, val_dim = state.shape
    key_width, val_width = heads * key_dim, heads * val_dim
    vmem = pl.BlockSpec(memory_space=pltpu.VMEM)
    hbm = pl.BlockSpec(memory_space=pltpu.HBM)
    weights = (w_query, w_key, w_decay, w_value, w_gate, w_out, w_up, w_down)
    a_width = 3 * key_width + 128
    coef_rows = 3 * heads * seqs
    coef_rows += -coef_rows % 8
    dma = pltpu.SemaphoreType.DMA
    scratch = (
        [
            pltpu.VMEM(tokens.shape, bf16),
            pltpu.VMEM((2, 1, half), f32),
            pltpu.VMEM((1, key_width), f32),
            pltpu.VMEM((1, val_dim), f32),
            pltpu.VMEM((n_kv, 2, 1, half), f32),
        ]
        + [pltpu.VMEM(weight.shape, bf16) for weight in weights]
        + [
            pltpu.VMEM((2, rows, half), bf16),
            pltpu.VMEM((n_kv, seqs, a_width), bf16),
            pltpu.VMEM((n_kv, seqs, val_width), bf16),
            pltpu.VMEM((n_kv, seqs, val_width), bf16),
            pltpu.VMEM((n_kv - 1, seqs, a_width), bf16),
            pltpu.VMEM((n_kv - 1, seqs, val_width), bf16),
            pltpu.VMEM((n_kv - 1, seqs, val_width), bf16),
            pltpu.VMEM((coef_rows, key_dim), f32),
            pltpu.VMEM((key_dim, coef_rows), f32),
            pltpu.VMEM((seqs, val_width), f32),
            pltpu.VMEM((heads, seqs, val_dim), f32),
            pltpu.VMEM((n_kv, seqs, val_width), bf16),
            pltpu.VMEM((rows, val_width), f32),
            pltpu.VMEM((2, rows, half), f32),
            pltpu.VMEM((2, rows, half), f32),
            pltpu.VMEM((n_kv, 2, rows, half), bf16),
            pltpu.VMEM((2 * n_kv - 1, rows, half), bf16),
            pltpu.VMEM((2 * n_kv - 1, rows, half), bf16),
            dma((14,)),
            dma((2,)),
            dma((3, n_kv - 1)),
            dma((3, n_kv - 1)),
            dma((n_kv - 1,)),
            dma((n_kv - 1,)),
            dma((2,)),
            dma((n_kv - 1,)),
            dma((n_kv - 1,)),
            dma((2 * n_kv - 1,)),
            dma((2 * n_kv - 1,)),
        ]
    )
    mixed, new_state = pl.pallas_call(
        functools.partial(layer_kernel, n_kv),
        out_shape=(
            pltpu.VMEM(tokens.shape, bf16),
            pltpu.VMEM(state.shape, f32),
        ),
        in_specs=[hbm] * 14,
        out_specs=(vmem, vmem),
        scratch_shapes=scratch,
        compiler_params=pltpu.CompilerParams(
            collective_id=0, has_side_effects=True, vmem_limit_bytes=VMEM_BYTES - 4 * state.size - 2**19
        ),
    )(
        tokens,
        mix_gain.reshape(2, 1, half),
        decay_offset.reshape(1, key_width),
        head_gain.reshape(1, val_dim),
        mlp_gain.reshape(n_kv, 2, 1, half),
        state,
        *weights,
    )
    return pl.pallas_call(
        write_kernel,
        out_shape=(
            jax.ShapeDtypeStruct(tokens.shape, bf16),
            jax.ShapeDtypeStruct(state.shape, f32),
        ),
        in_specs=[vmem] * 2,
        out_specs=(hbm, hbm),
        scratch_shapes=[dma((seqs, heads)), dma((1,))],
        compiler_params=pltpu.CompilerParams(vmem_limit_bytes=2**20),
    )(
        pltpu.with_memory_space_constraint(mixed, pltpu.VMEM),
        pltpu.with_memory_space_constraint(new_state, pltpu.VMEM),
    )


def fits_kernel(mesh):
    n_kv, n_tp = mesh.shape["kv"], mesh.shape["tp"]
    return n_tp == 2 and n_kv > 1 and D % (128 * n_kv * n_tp) == 0


def solution(mesh):
    in_specs = (
        P("dp", ("kv", "tp")),
        P(("dp", "kv"), "tp", None, None),
        P("kv"),
        P("kv", "tp"),
        P("kv", "tp"),
        P("kv", "tp"),
        P("kv", "tp"),
        P("kv", "tp"),
        P("tp"),
        P(),
        P("tp", "kv"),
        P(),
        P(None, ("kv", "tp")),
        P(("kv", "tp"), None),
    )
    out_specs = (P("dp", ("kv", "tp")), P(("dp", "kv"), "tp", None, None))
    shards = plain_shards
    if fits_kernel(mesh):
        shards = functools.partial(kernel_shards, mesh.shape["kv"])
    return jax.shard_map(shards, mesh=mesh, in_specs=in_specs, out_specs=out_specs, check_vma=False)
```

profile of v0, /device:TPU:0, one launch (start us, length us, event | category | flops | bytes accessed | tf_op | source)
XLA Modules:
  0.0 28.2 jit_solution(12248526052322322839)
XLA Ops:
  0.6 25.5 %shard_map.149 = (bf16[16,256]{1,0:T(8,128)(2,1)S(1)}, f32[4,2,256,512]{3,2,1,0:T(8,128)S(1)}) custom-call(bf16[16,256]{1,0:T(8,128)(2,1)} %tok_hbm.1, f32[2,1,256]{2,1,0:T(1,128)} %bitcast.5, f32[1,512]{1,0:T(1,128)} %bitcast.6, f32[1,512]{1,0:T(1,128)} %bitcast.7, f32[4,2,1,256]{3,2,1,0:T(1,128)} %bitcast.4, f32[4,2,256,512]{3,2,1,0:T(8,128)} %state_hbm.1, ...), custom_call_target="tpu_custom_call" | custom-call | tf_op jit(solution)/shard_map/pallas_call | solution.py:521
  26.1 2.1 %shard_map.150 = (bf16[16,256]{1,0:T(8,128)(2,1)}, f32[4,2,256,512]{3,2,1,0:T(8,128)}) custom-call(bf16[16,256]{1,0:T(8,128)(2,1)S(1)} %get-tuple-element.4.mixed_ref, f32[4,2,256,512]{3,2,1,0:T(8,128)S(1)} %get-tuple-element.5.state_ref), custom_call_target="tpu_custom_call" | custom-call | tf_op jit(solution)/shard_map/pallas_call | solution.py:542
where the time goes:
time: 28.4 us; the launch traced here: 28.2 us
  Pallas kernels  27.6 us (97%)
  between operations  0.64 us (2%)
    pallas_call x1, Pallas kernels, kernel_shards(): pl.pallas_call(functools.partial(layer_kernel, n_kv), out_shape=(pltpu.VM...  25.5 us
    pallas_call x1, Pallas kernels, kernel_shards(): pl.pallas_call(write_kernel, out_shape=(jax.ShapeDtypeStruct(tokens.shape...  2.08 us

commit v1 on v0

--- a/solution.py
+++ b/solution.py
@@ -103,6 +103,20 @@
 VMEM_BYTES = 67_043_328
 
 
+def pick(index, values):
+    chosen = values[0]
+    for at in range(1, len(values)):
+        chosen = jnp.where(index == at, values[at], chosen)
+    return chosen
+
+
+def far_first(n_kv, kv):
+    orders = [
+        sorted((j for j in range(n_kv) if j != me), key=lambda j: (-abs(j - me), j)) for me in range(n_kv)
+    ]
+    return [pick(kv, [order[at] for order in orders]) for at in range(n_kv - 1)]
+
+
 def layer_kernel(
     n_kv,
     tok_hbm,
@@ -134,6 +148,7 @@
     w_out_ref,
     w_up_ref,
     w_down_ref,
+    w_out_other,
     tok_all,
     send_a,
     send_b,
@@ -147,18 +162,19 @@
     read,
     gated_all,
     gated_rows,
-    branch_own,
-    branch_other,
     stream_all,
     down_send,
+    down_own,
     down_recv,
     load_sem,
+    pair_sem,
+    go_sem,
     tok_sem,
+    w_out_sem,
     proj_send_sem,
     proj_recv_sem,
     gated_send_sem,
     gated_recv_sem,
-    branch_sem,
     stream_send_sem,
     stream_recv_sem,
     down_send_sem,
@@ -171,18 +187,30 @@
     seqs, heads, key_dim, val_dim = state_ref.shape
     key_width, val_width = heads * key_dim, heads * val_dim
     width = 2 * n_kv * half
-
-    def peer(offset):
-        return lax.rem(kv + offset, n_kv)
+    far = far_first(n_kv, kv)
+    near = far[::-1]
+
+    def remote(src, dst, send_sem, recv_sem, to_kv, to_tp):
+        return pltpu.make_async_remote_copy(
+            src_ref=src,
+            dst_ref=dst,
+            send_sem=send_sem,
+            recv_sem=recv_sem,
+            device_id={"kv": to_kv, "tp": to_tp},
+            device_id_type=MESH,
+        )
+
+    def signal(sem, to_kv, to_tp):
+        pl.semaphore_signal(sem, inc=1, device_id={"kv": to_kv, "tp": to_tp}, device_id_type=MESH)
 
     barrier = pltpu.get_barrier_semaphore()
-    for offset in range(n_kv):
-        for to_tp in (tp, other):
-            if offset == 0 and to_tp is tp:
-                continue
-            pl.semaphore_signal(
-                barrier, inc=1, device_id={"kv": peer(offset), "tp": to_tp}, device_id_type=MESH
-            )
+
+    @pl.when(tp == 1)
+    def _():
+        signal(barrier, kv, 0)
+
+    for j in far:
+        signal(barrier, j, 1)
 
     loads = {}
     for at, (name, source, target) in enumerate(
@@ -198,31 +226,40 @@
             ("head_gain", head_gain_hbm, head_gain_ref),
             ("mlp_gain", mlp_gain_hbm, mlp_gain_ref),
             ("state", state_hbm, state_ref),
-            ("out", w_out_hbm, w_out_ref),
             ("up", w_up_hbm, w_up_ref),
             ("down", w_down_hbm, w_down_ref),
+            ("out", w_out_hbm, w_out_ref),
         )
     ):
         loads[name] = pltpu.make_async_copy(source, target, load_sem.at[at])
-        loads[name].start()
+        if name != "out":
+            loads[name].start()
+
+    @pl.when(tp == 0)
+    def _():
+        pl.semaphore_wait(barrier, 1)
+        signal(pair_sem, kv, 1)
+
+    @pl.when(tp == 1)
+    def _():
+        loads["out"].start()
+        pl.semaphore_wait(pair_sem, 1)
+
     loads["tokens"].wait()
-    pl.semaphore_wait(barrier, 2 * n_kv - 1)
-
-    tok_copy = pltpu.make_async_remote_copy(
-        src_ref=tok_ref,
-        dst_ref=tok_all.at[tp],
-        send_sem=tok_sem.at[0],
-        recv_sem=tok_sem.at[1],
-        device_id={"kv": kv, "tp": other},
-        device_id_type=MESH,
-    )
+    tok_copy = remote(tok_ref, tok_all.at[tp], tok_sem.at[0], tok_sem.at[1], kv, other)
     tok_copy.start()
+    tok_all[tp] = tok_ref[...]
     tok_own = tok_ref[...].astype(f32)
     squares = jnp.sum(tok_own * tok_own, axis=1, keepdims=True)
     for name in ("mix_gain", "offset", "head_gain", "mlp_gain"):
         loads[name].wait()
     tok_copy.wait_recv()
-    tok_all[tp] = tok_ref[...]
+
+    @pl.when(tp == 1)
+    def _():
+        pl.semaphore_wait(barrier, 2 * (n_kv - 1))
+        signal(go_sem, kv, 0)
+
     tok_other = tok_all[other].astype(f32)
     squares = squares + jnp.sum(tok_other * tok_other, axis=1, keepdims=True)
     scaled = jnp.concatenate(
@@ -236,20 +273,17 @@
         for owner in range(n_kv):
             send[owner, :, at : at + columns] = total[owner * seqs : (owner + 1) * seqs].astype(bf16)
 
-    def send_group(group, send, recv):
-        copies = []
-        for offset in reversed(range(1, n_kv)):
-            copy = pltpu.make_async_remote_copy(
-                src_ref=send.at[peer(offset)],
-                dst_ref=recv.at[offset - 1],
-                send_sem=proj_send_sem.at[group, offset - 1],
-                recv_sem=proj_recv_sem.at[group, offset - 1],
-                device_id={"kv": peer(offset), "tp": tp},
-                device_id_type=MESH,
-            )
-            copy.start()
-            copies.append(copy)
-        return copies
+    groups = ((send_a, recv_a), (send_b, recv_b), (send_c, recv_c))
+
+    def proj_copy(group, j, slot):
+        send, recv = groups[group]
+        return remote(
+            send.at[j], recv.at[slot], proj_send_sem.at[group, j], proj_recv_sem.at[group, slot], j, tp
+        )
+
+    def send_group(group):
+        for j in far:
+            proj_copy(group, j, kv).start()
 
     wide = jnp.broadcast_to(squares, (rows, 128))
     lane = lax.broadcasted_iota(jnp.int32, (seqs, 128), 1)
@@ -261,21 +295,33 @@
     project("q", wq_ref, send_a, 0)
     project("k", wk_ref, send_a, key_width)
     project("d", wd_ref, send_a, 2 * key_width)
-    copies_a = send_group(0, send_a, recv_a)
+
+    @pl.when(tp == 0)
+    def _():
+        pl.semaphore_wait(go_sem, 1)
+
+    send_group(0)
     project("v", wv_ref, send_b, 0)
-    copies_b = send_group(1, send_b, recv_b)
+    send_group(1)
     project("g", wg_ref, send_c, 0)
-    copies_c = send_group(2, send_c, recv_c)
-
-    def gathered(copies, send, recv):
+    send_group(2)
+
+    w_out_copy = remote(w_out_hbm, w_out_other, w_out_sem.at[0], w_out_sem.at[1], kv, 1)
+
+    @pl.when(tp == 0)
+    def _():
+        w_out_copy.start()
+
+    def gathered(group):
+        send, recv = groups[group]
         total = send[kv].astype(f32)
-        for copy in copies:
-            copy.wait_recv()
-        for offset in range(n_kv - 1):
-            total = total + recv[offset].astype(f32)
+        for j in near:
+            proj_copy(group, j, j).wait_recv()
+        for j in near:
+            total = total + recv[j].astype(f32)
         return total
 
-    group_a = gathered(copies_a, send_a, recv_a)
+    group_a = gathered(0)
     row_sums = group_a[:, 3 * key_width : 3 * key_width + 1] + group_a[:, 3 * key_width + 64 : 3 * key_width + 65]
     row_scale = lax.rsqrt(row_sums * (1.0 / width) + epsilon)
     queries = group_a[:, :key_width] * (row_scale * key_dim**-0.5)
@@ -302,31 +348,31 @@
                 total = total + jnp.sum(product.reshape(ROW_CHUNK // 8, 8, val_dim), axis=0)
             read[h, b : b + 1, :] = jnp.sum(total, axis=0, keepdims=True)
 
-    values = gathered(copies_b, send_b, recv_b) * row_scale
+    values = gathered(1) * row_scale
     vals[...] = values
-    gates = gathered(copies_c, send_c, recv_c) * row_scale
+    gates = gathered(2) * row_scale
     for h in range(heads):
         cols = slice(h * val_dim, (h + 1) * val_dim)
         dots = jnp.sum(overlap[:, h * key_dim : (h + 1) * key_dim], axis=1, keepdims=True)
         readout = read[h] + dots * values[:, cols]
         mean = jnp.mean(readout * readout, axis=1, keepdims=True)
         gate = gates[:, cols]
-        gated_all[kv, :, cols] = (
+        gated_all[tp, kv, :, cols] = (
             readout * lax.rsqrt(mean + epsilon) * head_gain_ref[...] * (gate * jax.nn.sigmoid(gate))
         ).astype(bf16)
 
-    gated_copies = []
-    for offset in range(1, n_kv):
-        copy = pltpu.make_async_remote_copy(
-            src_ref=gated_all.at[kv],
-            dst_ref=gated_all.at[kv],
-            send_sem=gated_send_sem.at[offset - 1],
-            recv_sem=gated_recv_sem.at[offset - 1],
-            device_id={"kv": peer(offset), "tp": tp},
-            device_id_type=MESH,
+    def gated_copy(j, from_tp, from_kv):
+        block = gated_all.at[from_tp, from_kv]
+        return remote(
+            block, block, gated_send_sem.at[j], gated_recv_sem.at[from_tp, from_kv], j, 1
         )
-        copy.start()
-        gated_copies.append(copy)
+
+    for j in far:
+        gated_copy(j, tp, kv).start()
+
+    @pl.when(tp == 0)
+    def _():
+        gated_copy(kv, 0, kv).start()
 
     for h in range(heads):
         for b in range(seqs):
@@ -339,46 +385,53 @@
                     + coef_t[piece, at + seqs : at + seqs + 1] * value_row
                 )
 
-    for copy in gated_copies:
-        copy.wait_recv()
-    for owner in range(n_kv):
-        gated_rows[owner * seqs : (owner + 1) * seqs, :] = gated_all[owner].astype(f32)
-    loads["out"].wait()
-    branch = jnp.dot(gated_rows[...].astype(bf16), w_out_ref[...], preferred_element_type=f32)
-    for i in range(2):
-        branch_own[i] = branch[:, i * half : (i + 1) * half]
-    branch_copy = pltpu.make_async_remote_copy(
-        src_ref=branch_own,
-        dst_ref=branch_other,
-        send_sem=branch_sem.at[0],
-        recv_sem=branch_sem.at[1],
-        device_id={"kv": kv, "tp": other},
-        device_id_type=MESH,
-    )
-    branch_copy.start()
-    branch_copy.wait_recv()
-    for i in range(2):
-        stream_all[kv, i] = (tok_all[i].astype(f32) + (branch_own[i] + branch_other[i])).astype(bf16)
-    stream_copies = []
-    for offset in range(1, n_kv):
-        copy = pltpu.make_async_remote_copy(
-            src_ref=stream_all.at[kv],
-            dst_ref=stream_all.at[kv],
-            send_sem=stream_send_sem.at[offset - 1],
-            recv_sem=stream_recv_sem.at[offset - 1],
-            device_id={"kv": peer(offset), "tp": tp},
-            device_id_type=MESH,
-        )
-        copy.start()
-        stream_copies.append(copy)
+    tok_copy.wait_send()
+    for group in range(3):
+        for j in far:
+            proj_copy(group, j, kv).wait_send()
+
+    def stream_copy(j, to_tp, owner):
+        block = stream_all.at[owner]
+        return remote(block, block, stream_send_sem.at[j, to_tp], stream_recv_sem.at[owner], j, to_tp)
+
+    def out_rows(from_tp):
+        for owner in range(n_kv):
+            gated_rows[owner * seqs : (owner + 1) * seqs, :] = gated_all[from_tp, owner].astype(f32)
+        return gated_rows[...].astype(bf16)
+
+    @pl.when(tp == 1)
+    def _():
+        for j in near:
+            gated_copy(kv, 1, j).wait_recv()
+        loads["out"].wait()
+        branch = jnp.dot(out_rows(1), w_out_ref[...], preferred_element_type=f32)
+        w_out_copy.wait_recv()
+        for j in [kv] + near:
+            gated_copy(kv, 0, j).wait_recv()
+        branch = branch + jnp.dot(out_rows(0), w_out_other[...], preferred_element_type=f32)
+        for i in range(2):
+            stream_all[kv, i] = (tok_all[i].astype(f32) + branch[:, i * half : (i + 1) * half]).astype(bf16)
+        for j in far:
+            for to_tp in range(2):
+                stream_copy(j, to_tp, kv).start()
+        stream_copy(kv, 0, kv).start()
+
+    for j in far:
+        gated_copy(j, tp, kv).wait_send()
 
     loads["up"].wait()
+
+    @pl.when(tp == 0)
+    def _():
+        gated_copy(kv, 0, kv).wait_send()
+        w_out_copy.wait_send()
+        stream_copy(kv, 0, kv).wait_recv()
+
     hidden = None
     sums = None
-    for step in UP_ORDER(n_kv):
+    for step, owner in enumerate([kv] + near):
         if step > 0:
-            stream_copies[step - 1].wait_recv()
-        owner = lax.rem(kv + n_kv - step, n_kv)
+            stream_copy(kv, tp, owner).wait_recv()
         pieces = [stream_all[owner, i].astype(f32) for i in range(2)]
         normed = jnp.concatenate(
             [(piece * mlp_gain_ref[owner, i]).astype(bf16) for i, piece in enumerate(pieces)], axis=1
@@ -388,47 +441,48 @@
         part = sum(jnp.sum(piece * piece, axis=1, keepdims=True) for piece in pieces)
         hidden = term if hidden is None else hidden + term
         sums = part if sums is None else sums + part
+        if step == 0:
+            loads["down"].wait()
     mlp_scale = lax.rsqrt(sums * (1.0 / width) + epsilon)
     active = jnp.maximum(hidden * mlp_scale, 0.0)
     squared = (active * active).astype(bf16)
 
-    loads["down"].wait()
-
-    def down_columns(offset, to_tp):
-        block = peer(offset) * 2 + to_tp
-        first = pl.multiple_of(block * half, half)
-        return jnp.dot(squared, w_down_ref[:, pl.ds(first, half)], preferred_element_type=f32)
-
-    down_copies = []
-    for offset in UP_ORDER(n_kv)[::-1]:
-        for flip in (1, 0):
-            if offset == 0 and flip == 0:
-                continue
-            to_tp = other if flip else tp
-            slot = offset * 2 + flip - 1
-            down_send[slot] = down_columns(offset, to_tp).astype(bf16)
-            copy = pltpu.make_async_remote_copy(
-                src_ref=down_send.at[slot],
-                dst_ref=down_recv.at[slot],
-                send_sem=down_send_sem.at[slot],
-                recv_sem=down_recv_sem.at[slot],
-                device_id={"kv": peer(offset), "tp": to_tp},
-                device_id_type=MESH,
-            )
-            copy.start()
-            down_copies.append((slot, copy))
-    total = stream_all[kv, tp].astype(f32) + down_columns(0, tp)
-    for slot, copy in down_copies:
-        copy.wait_recv()
+    def down_copy(at, j, to_tp, slot):
+        return remote(
+            down_send.at[at, to_tp], down_recv.at[slot], down_send_sem.at[at, to_tp], down_recv_sem.at[slot], j, to_tp
+        )
+
+    me = 2 * kv + tp
+    for at, j in enumerate(far + [kv]):
+        first = pl.multiple_of(j * (2 * half), 2 * half)
+        term = jnp.dot(squared, w_down_ref[:, pl.ds(first, 2 * half)], preferred_element_type=f32)
+        for i in range(2):
+            down_send[at, i] = term[:, i * half : (i + 1) * half].astype(bf16)
+            if at == n_kv - 1:
+                down_own[i] = term[:, i * half : (i + 1) * half]
+        if at < n_kv - 1:
+            for i in range(2):
+                down_copy(at, j, i, me).start()
+        else:
+            down_copy(at, kv, other, me).start()
+    total = stream_all[kv, tp].astype(f32) + down_own[tp]
+
+    @pl.when(tp == 1)
+    def _():
+        for j in far:
+            for to_tp in range(2):
+                stream_copy(j, to_tp, kv).wait_send()
+        stream_copy(kv, 0, kv).wait_send()
+
+    slots = [2 * kv + other] + [2 * j + i for j in near for i in range(2)]
+    for slot in slots:
+        down_copy(0, kv, tp, slot).wait_recv()
         total = total + down_recv[slot].astype(f32)
     mixed_ref[...] = total.astype(bf16)
-
-    tok_copy.wait_send()
-    branch_copy.wait_send()
-    for copy in copies_a + copies_b + copies_c + gated_copies + stream_copies:
-        copy.wait_send()
-    for _, copy in down_copies:
-        copy.wait_send()
+    for at, j in enumerate(far):
+        for i in range(2):
+            down_copy(at, j, i, me).wait_send()
+    down_copy(n_kv - 1, kv, other, me).wait_send()
 
 
 def write_kernel(mixed_ref, state_ref, mixed_hbm, state_hbm, state_sem, mixed_sem):
@@ -443,10 +497,6 @@
         copy.start()
     for copy in copies:
         copy.wait()
-
-
-def UP_ORDER(n_kv):
-    return sorted(range(n_kv), key=lambda offset: min(offset, n_kv - offset))
 
 
 def kernel_shards(
@@ -477,6 +527,7 @@
     coef_rows = 3 * heads * seqs
     coef_rows += -coef_rows % 8
     dma = pltpu.SemaphoreType.DMA
+    regular = pltpu.SemaphoreType.REGULAR
     scratch = (
         [
             pltpu.VMEM(tokens.shape, bf16),
@@ -487,35 +538,37 @@
         ]
         + [pltpu.VMEM(weight.shape, bf16) for weight in weights]
         + [
+            pltpu.VMEM(w_out.shape, bf16),
             pltpu.VMEM((2, rows, half), bf16),
             pltpu.VMEM((n_kv, seqs, a_width), bf16),
             pltpu.VMEM((n_kv, seqs, val_width), bf16),
             pltpu.VMEM((n_kv, seqs, val_width), bf16),
-            pltpu.VMEM((n_kv - 1, seqs, a_width), bf16),
-            pltpu.VMEM((n_kv - 1, seqs, val_width), bf16),
-            pltpu.VMEM((n_kv - 1, seqs, val_width), bf16),
+            pltpu.VMEM((n_kv, seqs, a_width), bf16),
+            pltpu.VMEM((n_kv, seqs, val_width), bf16),
+            pltpu.VMEM((n_kv, seqs, val_width), bf16),
             pltpu.VMEM((coef_rows, key_dim), f32),
             pltpu.VMEM((key_dim, coef_rows), f32),
             pltpu.VMEM((seqs, val_width), f32),
             pltpu.VMEM((heads, seqs, val_dim), f32),
-            pltpu.VMEM((n_kv, seqs, val_width), bf16),
+            pltpu.VMEM((2, n_kv, seqs, val_width), bf16),
             pltpu.VMEM((rows, val_width), f32),
+            pltpu.VMEM((n_kv, 2, rows, half), bf16),
+            pltpu.VMEM((n_kv, 2, rows, half), bf16),
             pltpu.VMEM((2, rows, half), f32),
-            pltpu.VMEM((2, rows, half), f32),
-            pltpu.VMEM((n_kv, 2, rows, half), bf16),
-            pltpu.VMEM((2 * n_kv - 1, rows, half), bf16),
-            pltpu.VMEM((2 * n_kv - 1, rows, half), bf16),
+            pltpu.VMEM((2 * n_kv, rows, half), bf16),
             dma((14,)),
+            regular,
+            regular,
             dma((2,)),
-            dma((3, n_kv - 1)),
-            dma((3, n_kv - 1)),
-            dma((n_kv - 1,)),
-            dma((n_kv - 1,)),
             dma((2,)),
-            dma((n_kv - 1,)),
-            dma((n_kv - 1,)),
-            dma((2 * n_kv - 1,)),
-            dma((2 * n_kv - 1,)),
+            dma((3, n_kv)),
+            dma((3, n_kv)),
+            dma((n_kv,)),
+            dma((2, n_kv)),
+            dma((n_kv, 2)),
+            dma((n_kv,)),
+            dma((n_kv, 2)),
+            dma((2 * n_kv,)),
         ]
     )
     mixed, new_state = pl.pallas_call(

time: 28.4 us -> 24.8 us (0.87)
  Pallas kernels: 27.6 us -> 24 us
    pallas_call x1, Pallas kernels: 25.5 us -> 21.9 us  [kernel_shards(): pl.pallas_call(functools.partial(layer_kernel, n_kv), out_shape=(pltpu.VM...]
where the time goes in v1:
time: 24.8 us; the launch traced here: 24.6 us
  Pallas kernels  24 us (97%)
  between operations  0.64 us (3%)
    pallas_call x1, Pallas kernels, kernel_shards(): pl.pallas_call(functools.partial(layer_kernel, n_kv), out_shape=(pltpu.VM...  21.9 us
    pallas_call x1, Pallas kernels, kernel_shards(): pl.pallas_call(write_kernel, out_shape=(jax.ShapeDtypeStruct(tokens.shape...  2.08 us

profile of v1, /device:TPU:0, one launch (start us, length us, event | category | flops | bytes accessed | tf_op | source)
XLA Modules:
  0.0 24.6 jit_solution(15707793899552836399)
XLA Ops:
  0.6 21.9 %shard_map.149 = (bf16[16,256]{1,0:T(8,128)(2,1)S(1)}, f32[4,2,256,512]{3,2,1,0:T(8,128)S(1)}) custom-call(bf16[16,256]{1,0:T(8,128)(2,1)} %tok_hbm.1, f32[2,1,256]{2,1,0:T(1,128)} %bitcast.5, f32[1,512]{1,0:T(1,128)} %bitcast.6, f32[1,512]{1,0:T(1,128)} %bitcast.7, f32[4,2,1,256]{3,2,1,0:T(1,128)} %bitcast.4, f32[4,2,256,512]{3,2,1,0:T(8,128)} %state_hbm.1, ...), custom_call_target="tpu_custom_call" | custom-call | tf_op jit(solution)/shard_map/pallas_call | solution.py:574
  22.5 2.1 %shard_map.150 = (bf16[16,256]{1,0:T(8,128)(2,1)}, f32[4,2,256,512]{3,2,1,0:T(8,128)}) custom-call(bf16[16,256]{1,0:T(8,128)(2,1)S(1)} %get-tuple-element.4.mixed_ref, f32[4,2,256,512]{3,2,1,0:T(8,128)S(1)} %get-tuple-element.5.state_ref), custom_call_target="tpu_custom_call" | custom-call | tf_op jit(solution)/shard_map/pallas_call | solution.py:595

commit v2 on v1

--- a/solution.py
+++ b/solution.py
@@ -140,9 +140,7 @@
     decay_offset_ref,
     head_gain_ref,
     mlp_gain_ref,
-    wq_ref,
-    wk_ref,
-    wd_ref,
+    w_qkd_ref,
     wv_ref,
     wg_ref,
     w_out_ref,
@@ -167,18 +165,14 @@
     down_own,
     down_recv,
     load_sem,
-    pair_sem,
-    go_sem,
+    ready_sem,
     tok_sem,
     w_out_sem,
-    proj_send_sem,
-    proj_recv_sem,
-    gated_send_sem,
-    gated_recv_sem,
+    proj_sem,
+    gated_sem,
     stream_send_sem,
     stream_recv_sem,
-    down_send_sem,
-    down_recv_sem,
+    down_sem,
 ):
     f32, bf16 = jnp.float32, jnp.bfloat16
     kv, tp = lax.axis_index("kv"), lax.axis_index("tp")
@@ -212,38 +206,44 @@
     for j in far:
         signal(barrier, j, 1)
 
+        @pl.when(j > kv)
+        def _():
+            signal(barrier, j, 0)
+
     loads = {}
-    for at, (name, source, target) in enumerate(
-        (
-            ("tokens", tok_hbm, tok_ref),
-            ("mix_gain", mix_gain_hbm, mix_gain_ref),
-            ("q", wq_hbm, wq_ref),
-            ("k", wk_hbm, wk_ref),
-            ("d", wd_hbm, wd_ref),
-            ("v", wv_hbm, wv_ref),
-            ("g", wg_hbm, wg_ref),
-            ("offset", decay_offset_hbm, decay_offset_ref),
-            ("head_gain", head_gain_hbm, head_gain_ref),
-            ("mlp_gain", mlp_gain_hbm, mlp_gain_ref),
-            ("state", state_hbm, state_ref),
-            ("up", w_up_hbm, w_up_ref),
-            ("down", w_down_hbm, w_down_ref),
-            ("out", w_out_hbm, w_out_ref),
-        )
+    at_sem = {}
+    for name, source, target in (
+        ("tokens", tok_hbm, tok_ref),
+        ("mix_gain", mix_gain_hbm, mix_gain_ref),
+        ("q", wq_hbm, w_qkd_ref.at[0]),
+        ("k", wk_hbm, w_qkd_ref.at[1]),
+        ("d", wd_hbm, w_qkd_ref.at[2]),
+        ("offset", decay_offset_hbm, decay_offset_ref),
+        ("head_gain", head_gain_hbm, head_gain_ref),
+        ("mlp_gain", mlp_gain_hbm, mlp_gain_ref),
+        ("v", wv_hbm, wv_ref),
+        ("g", wg_hbm, wg_ref),
+        ("state", state_hbm, state_ref),
+        ("up", w_up_hbm, w_up_ref),
+        ("down", w_down_hbm, w_down_ref),
+        ("out", w_out_hbm, w_out_ref),
     ):
-        loads[name] = pltpu.make_async_copy(source, target, load_sem.at[at])
+        group = "q" if name in ("k", "d") else name
+        sem = load_sem.at[at_sem.setdefault(group, len(at_sem))]
+        loads[name] = pltpu.make_async_copy(source, target, sem)
         if name != "out":
             loads[name].start()
+    loads["q"] = pltpu.make_async_copy(w_qkd_ref, w_qkd_ref, load_sem.at[at_sem["q"]])
 
     @pl.when(tp == 0)
     def _():
-        pl.semaphore_wait(barrier, 1)
-        signal(pair_sem, kv, 1)
+        pl.semaphore_wait(barrier, 1 + 2 * kv)
+        signal(ready_sem, kv, 1)
 
     @pl.when(tp == 1)
     def _():
         loads["out"].start()
-        pl.semaphore_wait(pair_sem, 1)
+        pl.semaphore_wait(ready_sem, 1)
 
     loads["tokens"].wait()
     tok_copy = remote(tok_ref, tok_all.at[tp], tok_sem.at[0], tok_sem.at[1], kv, other)
@@ -251,39 +251,59 @@
     tok_all[tp] = tok_ref[...]
     tok_own = tok_ref[...].astype(f32)
     squares = jnp.sum(tok_own * tok_own, axis=1, keepdims=True)
-    for name in ("mix_gain", "offset", "head_gain", "mlp_gain"):
-        loads[name].wait()
+    loads["mix_gain"].wait()
+
+    def half_rows(which):
+        return pl.ds(pl.multiple_of(which * half, half), half)
+
+    scaled_own = (tok_own * mix_gain_ref[tp]).astype(bf16)
+    loads["q"].wait()
+    early = [
+        jnp.dot(scaled_own, w_qkd_ref[i, half_rows(tp), :], preferred_element_type=f32) for i in range(3)
+    ]
     tok_copy.wait_recv()
-
-    @pl.when(tp == 1)
-    def _():
-        pl.semaphore_wait(barrier, 2 * (n_kv - 1))
-        signal(go_sem, kv, 0)
-
     tok_other = tok_all[other].astype(f32)
     squares = squares + jnp.sum(tok_other * tok_other, axis=1, keepdims=True)
-    scaled = jnp.concatenate(
-        [(tok_all[i].astype(f32) * mix_gain_ref[i]).astype(bf16) for i in range(2)], axis=1
-    )
-
-    def project(name, weight_ref, send, at):
-        loads[name].wait()
-        total = jnp.dot(scaled, weight_ref[...], preferred_element_type=f32)
+    scaled_other = (tok_other * mix_gain_ref[other]).astype(bf16)
+
+    groups = ((send_a, recv_a), (send_b, recv_b), (send_c, recv_c))
+
+    def fill(send, total, at):
         columns = total.shape[1]
         for owner in range(n_kv):
             send[owner, :, at : at + columns] = total[owner * seqs : (owner + 1) * seqs].astype(bf16)
 
-    groups = ((send_a, recv_a), (send_b, recv_b), (send_c, recv_c))
-
-    def proj_copy(group, j, slot):
+    def project(name, weight_ref, send):
+        loads[name].wait()
+        total = jnp.dot(scaled_own, weight_ref[half_rows(tp), :], preferred_element_type=f32)
+        fill(send, total + jnp.dot(scaled_other, weight_ref[half_rows(other), :], preferred_element_type=f32), 0)
+
+    def proj_copy(group, j):
         send, recv = groups[group]
-        return remote(
-            send.at[j], recv.at[slot], proj_send_sem.at[group, j], proj_recv_sem.at[group, slot], j, tp
+        return remote(send.at[j], recv.at[kv], proj_sem.at[group, 0], proj_sem.at[group, 1], j, tp)
+
+    def proj_all(group):
+        send, recv = groups[group]
+        some = pl.ds(0, n_kv - 1)
+        return remote(send.at[some], recv.at[some], proj_sem.at[group, 0], proj_sem.at[group, 1], kv, other)
+
+    def send_lower(group):
+        for j in far:
+
+            @pl.when(j < kv)
+            def _():
+                proj_copy(group, j).start()
+
+    def send_higher():
+        order = sorted(
+            ((group, at) for group in range(3) for at in range(n_kv - 1)),
+            key=lambda item: item[1] * 2 + (0 if item[0] == 0 else 3),
         )
-
-    def send_group(group):
-        for j in far:
-            proj_copy(group, j, kv).start()
+        for group, at in order:
+
+            @pl.when(far[at] > kv)
+            def _():
+                proj_copy(group, far[at]).start()
 
     wide = jnp.broadcast_to(squares, (rows, 128))
     lane = lax.broadcasted_iota(jnp.int32, (seqs, 128), 1)
@@ -292,21 +312,30 @@
         high = wide[mine].astype(bf16).astype(f32)
         sums = jnp.where(lane < 64, high, wide[mine] - high)
         send_a[owner, :, 3 * key_width :] = sums.astype(bf16)
-    project("q", wq_ref, send_a, 0)
-    project("k", wk_ref, send_a, key_width)
-    project("d", wd_ref, send_a, 2 * key_width)
+    late = [
+        jnp.dot(scaled_other, w_qkd_ref[i, half_rows(other), :], preferred_element_type=f32) for i in range(3)
+    ]
+    for i in range(3):
+        fill(send_a, early[i] + late[i], i * key_width)
+    send_lower(0)
+    project("v", wv_ref, send_b)
+    send_lower(1)
+
+    @pl.when(tp == 1)
+    def _():
+        pl.semaphore_wait(barrier, 2 * (n_kv - 1))
+        signal(ready_sem, kv, 0)
+
+    project("g", wg_ref, send_c)
+    send_lower(2)
 
     @pl.when(tp == 0)
     def _():
-        pl.semaphore_wait(go_sem, 1)
-
-    send_group(0)
-    project("v", wv_ref, send_b, 0)
-    send_group(1)
-    project("g", wg_ref, send_c, 0)
-    send_group(2)
-
-    w_out_copy = remote(w_out_hbm, w_out_other, w_out_sem.at[0], w_out_sem.at[1], kv, 1)
+        pl.semaphore_wait(ready_sem, 1)
+
+    send_higher()
+
+    w_out_copy = remote(w_out_hbm, w_out_other, w_out_sem, w_out_sem, kv, 1)
 
     @pl.when(tp == 0)
     def _():
@@ -315,8 +344,7 @@
     def gathered(group):
         send, recv = groups[group]
         total = send[kv].astype(f32)
-        for j in near:
-            proj_copy(group, j, j).wait_recv()
+        proj_all(group).wait_recv()
         for j in near:
             total = total + recv[j].astype(f32)
         return total
@@ -326,6 +354,7 @@
     row_scale = lax.rsqrt(row_sums * (1.0 / width) + epsilon)
     queries = group_a[:, :key_width] * (row_scale * key_dim**-0.5)
     new_keys = group_a[:, key_width : 2 * key_width] * row_scale
+    loads["offset"].wait()
     retain = jax.nn.sigmoid(
         group_a[:, 2 * key_width : 3 * key_width] * row_scale + decay_offset_ref[...]
     )
@@ -351,6 +380,7 @@
     values = gathered(1) * row_scale
     vals[...] = values
     gates = gathered(2) * row_scale
+    loads["head_gain"].wait()
     for h in range(heads):
         cols = slice(h * val_dim, (h + 1) * val_dim)
         dots = jnp.sum(overlap[:, h * key_dim : (h + 1) * key_dim], axis=1, keepdims=True)
@@ -361,18 +391,20 @@
             readout * lax.rsqrt(mean + epsilon) * head_gain_ref[...] * (gate * jax.nn.sigmoid(gate))
         ).astype(bf16)
 
-    def gated_copy(j, from_tp, from_kv):
-        block = gated_all.at[from_tp, from_kv]
-        return remote(
-            block, block, gated_send_sem.at[j], gated_recv_sem.at[from_tp, from_kv], j, 1
-        )
+    def gated_copy(j):
+        block = gated_all.at[tp, kv]
+        return remote(block, block, gated_sem.at[0], gated_sem.at[1 + tp], j, 1)
+
+    def gated_some(from_tp, count):
+        blocks = gated_all.at[from_tp, pl.ds(0, count)]
+        return remote(blocks, blocks, gated_sem.at[0], gated_sem.at[1 + from_tp], kv, other)
 
     for j in far:
-        gated_copy(j, tp, kv).start()
+        gated_copy(j).start()
 
     @pl.when(tp == 0)
     def _():
-        gated_copy(kv, 0, kv).start()
+        gated_copy(kv).start()
 
     for h in range(heads):
         for b in range(seqs):
@@ -387,12 +419,11 @@
 
     tok_copy.wait_send()
     for group in range(3):
-        for j in far:
-            proj_copy(group, j, kv).wait_send()
+        proj_all(group).wait_send()
 
     def stream_copy(j, to_tp, owner):
         block = stream_all.at[owner]
-        return remote(block, block, stream_send_sem.at[j, to_tp], stream_recv_sem.at[owner], j, to_tp)
+        return remote(block, block, stream_send_sem.at[to_tp], stream_recv_sem.at[owner], j, to_tp)
 
     def out_rows(from_tp):
         for owner in range(n_kv):
@@ -401,13 +432,11 @@
 
     @pl.when(tp == 1)
     def _():
-        for j in near:
-            gated_copy(kv, 1, j).wait_recv()
+        gated_some(1, n_kv - 1).wait_recv()
         loads["out"].wait()
         branch = jnp.dot(out_rows(1), w_out_ref[...], preferred_element_type=f32)
         w_out_copy.wait_recv()
-        for j in [kv] + near:
-            gated_copy(kv, 0, j).wait_recv()
+        gated_some(0, n_kv).wait_recv()
         branch = branch + jnp.dot(out_rows(0), w_out_other[...], preferred_element_type=f32)
         for i in range(2):
             stream_all[kv, i] = (tok_all[i].astype(f32) + branch[:, i * half : (i + 1) * half]).astype(bf16)
@@ -416,14 +445,14 @@
                 stream_copy(j, to_tp, kv).start()
         stream_copy(kv, 0, kv).start()
 
-    for j in far:
-        gated_copy(j, tp, kv).wait_send()
-
+        gated_some(1, n_kv - 1).wait_send()
+
+    loads["mlp_gain"].wait()
     loads["up"].wait()
 
     @pl.when(tp == 0)
     def _():
-        gated_copy(kv, 0, kv).wait_send()
+        gated_some(0, n_kv).wait_send()
         w_out_copy.wait_send()
         stream_copy(kv, 0, kv).wait_recv()
 
@@ -447,42 +476,44 @@
     active = jnp.maximum(hidden * mlp_scale, 0.0)
     squared = (active * active).astype(bf16)
 
-    def down_copy(at, j, to_tp, slot):
-        return remote(
-            down_send.at[at, to_tp], down_recv.at[slot], down_send_sem.at[at, to_tp], down_recv_sem.at[slot], j, to_tp
+    def down_copy(at, j, to_tp):
+        return remote(down_send.at[at, to_tp], down_recv.at[2 * kv + tp], down_sem.at[0], down_sem.at[1], j, to_tp)
+
+    def down_columns(first, columns):
+        return jnp.dot(
+            squared, w_down_ref[:, pl.ds(pl.multiple_of(first, half), columns)], preferred_element_type=f32
         )
 
-    me = 2 * kv + tp
-    for at, j in enumerate(far + [kv]):
-        first = pl.multiple_of(j * (2 * half), 2 * half)
-        term = jnp.dot(squared, w_down_ref[:, pl.ds(first, 2 * half)], preferred_element_type=f32)
-        for i in range(2):
-            down_send[at, i] = term[:, i * half : (i + 1) * half].astype(bf16)
-            if at == n_kv - 1:
-                down_own[i] = term[:, i * half : (i + 1) * half]
-        if at < n_kv - 1:
+    for at, j in enumerate(far):
+        if at == 0:
             for i in range(2):
-                down_copy(at, j, i, me).start()
+                down_send[at, i] = down_columns((2 * j + i) * half, half).astype(bf16)
+                down_copy(at, j, i).start()
         else:
-            down_copy(at, kv, other, me).start()
+            term = down_columns(2 * j * half, 2 * half)
+            for i in range(2):
+                down_send[at, i] = term[:, i * half : (i + 1) * half].astype(bf16)
+                down_copy(at, j, i).start()
+    term = down_columns(2 * kv * half, 2 * half)
+    for i in range(2):
+        down_own[i] = term[:, i * half : (i + 1) * half]
+        down_send[n_kv - 1, i] = term[:, i * half : (i + 1) * half].astype(bf16)
+    down_copy(n_kv - 1, kv, other).start()
     total = stream_all[kv, tp].astype(f32) + down_own[tp]
 
     @pl.when(tp == 1)
     def _():
-        for j in far:
-            for to_tp in range(2):
-                stream_copy(j, to_tp, kv).wait_send()
-        stream_copy(kv, 0, kv).wait_send()
-
-    slots = [2 * kv + other] + [2 * j + i for j in near for i in range(2)]
-    for slot in slots:
-        down_copy(0, kv, tp, slot).wait_recv()
+        remote(stream_all, stream_all, stream_send_sem.at[0], stream_recv_sem.at[0], kv, 0).wait_send()
+        some = stream_all.at[pl.ds(0, n_kv - 1)]
+        remote(some, some, stream_send_sem.at[1], stream_recv_sem.at[0], kv, 0).wait_send()
+
+    some = down_recv.at[pl.ds(0, 2 * n_kv - 1)]
+    down_all = remote(some, some, down_sem.at[0], down_sem.at[1], kv, other)
+    down_all.wait_recv()
+    for slot in [2 * kv + other] + [2 * j + i for j in near for i in range(2)]:
         total = total + down_recv[slot].astype(f32)
     mixed_ref[...] = total.astype(bf16)
-    for at, j in enumerate(far):
-        for i in range(2):
-            down_copy(at, j, i, me).wait_send()
-    down_copy(n_kv - 1, kv, other, me).wait_send()
+    down_all.wait_send()
 
 
 def write_kernel(mixed_ref, state_ref, mixed_hbm, state_hbm, state_sem, mixed_sem):
@@ -527,7 +558,6 @@
     coef_rows = 3 * heads * seqs
     coef_rows += -coef_rows % 8
     dma = pltpu.SemaphoreType.DMA
-    regular = pltpu.SemaphoreType.REGULAR
     scratch = (
         [
             pltpu.VMEM(tokens.shape, bf16),
@@ -536,7 +566,8 @@
             pltpu.VMEM((1, val_dim), f32),
             pltpu.VMEM((n_kv, 2, 1, half), f32),
         ]
-        + [pltpu.VMEM(weight.shape, bf16) for weight in weights]
+        + [pltpu.VMEM((3,) + w_query.shape, bf16)]
+        + [pltpu.VMEM(weight.shape, bf16) for weight in weights[3:]]
         + [
             pltpu.VMEM(w_out.shape, bf16),
             pltpu.VMEM((2, rows, half), bf16),
@@ -556,19 +587,15 @@
             pltpu.VMEM((n_kv, 2, rows, half), bf16),
             pltpu.VMEM((2, rows, half), f32),
             pltpu.VMEM((2 * n_kv, rows, half), bf16),
-            dma((14,)),
-            regular,
-            regular,
+            dma((12,)),
+            pltpu.SemaphoreType.REGULAR,
             dma((2,)),
+            dma,
+            dma((3, 2)),
+            dma((3,)),
             dma((2,)),
-            dma((3, n_kv)),
-            dma((3, n_kv)),
             dma((n_kv,)),
-            dma((2, n_kv)),
-            dma((n_kv, 2)),
-            dma((n_kv,)),
-            dma((n_kv, 2)),
-            dma((2 * n_kv,)),
+            dma((2,)),
         ]
     )
     mixed, new_state = pl.pallas_call(

time: 24.8 us -> 24.1 us (0.972)
  Pallas kernels: 24 us -> 23.3 us
    pallas_call x1, Pallas kernels: 21.9 us -> 21.2 us  [kernel_shards(): pl.pallas_call(functools.partial(layer_kernel, n_kv), out_shape=(pltpu.VM...]
where the time goes in v2:
time: 24.1 us; the launch traced here: 23.9 us
  Pallas kernels  23.3 us (97%)
  between operations  0.64 us (3%)
    pallas_call x1, Pallas kernels, kernel_shards(): pl.pallas_call(functools.partial(layer_kernel, n_kv), out_shape=(pltpu.VM...  21.2 us
    pallas_call x1, Pallas kernels, kernel_shards(): pl.pallas_call(write_kernel, out_shape=(jax.ShapeDtypeStruct(tokens.shape...  2.08 us

profile of v2, /device:TPU:0, one launch (start us, length us, event | category | flops | bytes accessed | tf_op | source)
XLA Modules:
  0.0 23.9 jit_solution(13326861289043239024)
XLA Ops:
  0.6 21.2 %shard_map.149 = (bf16[16,256]{1,0:T(8,128)(2,1)S(1)}, f32[4,2,256,512]{3,2,1,0:T(8,128)S(1)}) custom-call(bf16[16,256]{1,0:T(8,128)(2,1)} %tok_hbm.1, f32[2,1,256]{2,1,0:T(1,128)} %bitcast.5, f32[1,512]{1,0:T(1,128)} %bitcast.6, f32[1,512]{1,0:T(1,128)} %bitcast.7, f32[4,2,1,256]{3,2,1,0:T(1,128)} %bitcast.4, f32[4,2,256,512]{3,2,1,0:T(8,128)} %state_hbm.1, ...), custom_call_target="tpu_custom_call" | custom-call | tf_op jit(solution)/shard_map/pallas_call | solution.py:601
  21.8 2.1 %shard_map.150 = (bf16[16,256]{1,0:T(8,128)(2,1)}, f32[4,2,256,512]{3,2,1,0:T(8,128)}) custom-call(bf16[16,256]{1,0:T(8,128)(2,1)S(1)} %get-tuple-element.4.mixed_ref, f32[4,2,256,512]{3,2,1,0:T(8,128)S(1)} %get-tuple-element.5.state_ref), custom_call_target="tpu_custom_call" | custom-call | tf_op jit(solution)/shard_map/pallas_call | solution.py:622

commit v3 on v2

--- a/solution.py
+++ b/solution.py
@@ -147,6 +147,8 @@
     w_up_ref,
     w_down_ref,
     w_out_other,
+    w_up_other,
+    w_down_other,
     tok_all,
     send_a,
     send_b,
@@ -161,6 +163,7 @@
     gated_all,
     gated_rows,
     stream_all,
+    squared_ref,
     down_send,
     down_own,
     down_recv,
@@ -248,6 +251,21 @@
     loads["tokens"].wait()
     tok_copy = remote(tok_ref, tok_all.at[tp], tok_sem.at[0], tok_sem.at[1], kv, other)
     tok_copy.start()
+
+    w_out_copy = remote(w_out_hbm, w_out_other, w_out_sem.at[0], w_out_sem.at[0], kv, 1)
+    w_up_copy = remote(w_up_hbm, w_up_other, w_out_sem.at[1], w_out_sem.at[1], kv, 1)
+    w_down_copy = remote(
+        w_down_hbm.at[:, pl.ds(0, 2 * half)], w_down_other, w_out_sem.at[2], w_out_sem.at[2], kv, 1
+    )
+
+    @pl.when(tp == 0)
+    def _():
+        w_out_copy.start()
+
+    @pl.when((tp == 0) & (kv > 0))
+    def _():
+        w_up_copy.start()
+
     tok_all[tp] = tok_ref[...]
     tok_own = tok_ref[...].astype(f32)
     squares = jnp.sum(tok_own * tok_own, axis=1, keepdims=True)
@@ -334,12 +352,6 @@
         pl.semaphore_wait(ready_sem, 1)
 
     send_higher()
-
-    w_out_copy = remote(w_out_hbm, w_out_other, w_out_sem, w_out_sem, kv, 1)
-
-    @pl.when(tp == 0)
-    def _():
-        w_out_copy.start()
 
     def gathered(group):
         send, recv = groups[group]
@@ -406,6 +418,10 @@
     def _():
         gated_copy(kv).start()
 
+    @pl.when((tp == 0) & (kv > 0))
+    def _():
+        w_down_copy.start()
+
     for h in range(heads):
         for b in range(seqs):
             at = 3 * h * seqs + b
@@ -440,8 +456,8 @@
         branch = branch + jnp.dot(out_rows(0), w_out_other[...], preferred_element_type=f32)
         for i in range(2):
             stream_all[kv, i] = (tok_all[i].astype(f32) + branch[:, i * half : (i + 1) * half]).astype(bf16)
-        for j in far:
-            for to_tp in range(2):
+        for to_tp in (1, 0):
+            for j in far:
                 stream_copy(j, to_tp, kv).start()
         stream_copy(kv, 0, kv).start()
 
@@ -454,52 +470,93 @@
     def _():
         gated_some(0, n_kv).wait_send()
         w_out_copy.wait_send()
+
+        @pl.when(kv > 0)
+        def _():
+            w_up_copy.wait_send()
+            w_down_copy.wait_send()
+
         stream_copy(kv, 0, kv).wait_recv()
 
-    hidden = None
-    sums = None
-    for step, owner in enumerate([kv] + near):
-        if step > 0:
-            stream_copy(kv, tp, owner).wait_recv()
-        pieces = [stream_all[owner, i].astype(f32) for i in range(2)]
-        normed = jnp.concatenate(
-            [(piece * mlp_gain_ref[owner, i]).astype(bf16) for i, piece in enumerate(pieces)], axis=1
-        )
-        first = pl.multiple_of(owner * (2 * half), 2 * half)
-        term = jnp.dot(normed, w_up_ref[pl.ds(first, 2 * half), :], preferred_element_type=f32)
-        part = sum(jnp.sum(piece * piece, axis=1, keepdims=True) for piece in pieces)
-        hidden = term if hidden is None else hidden + term
-        sums = part if sums is None else sums + part
-        if step == 0:
-            loads["down"].wait()
-    mlp_scale = lax.rsqrt(sums * (1.0 / width) + epsilon)
-    active = jnp.maximum(hidden * mlp_scale, 0.0)
-    squared = (active * active).astype(bf16)
+    def hidden_units(weights_of, waits):
+        hidden = [None] * len(weights_of)
+        sums = None
+        for step, owner in enumerate([kv] + near):
+            for wait in waits[step]:
+                wait()
+            if step > 0:
+                stream_copy(kv, tp, owner).wait_recv()
+            pieces = [stream_all[owner, i].astype(f32) for i in range(2)]
+            normed = jnp.concatenate(
+                [(piece * mlp_gain_ref[owner, i]).astype(bf16) for i, piece in enumerate(pieces)], axis=1
+            )
+            first = pl.multiple_of(owner * (2 * half), 2 * half)
+            for at, ref in enumerate(weights_of):
+                term = jnp.dot(normed, ref[pl.ds(first, 2 * half), :], preferred_element_type=f32)
+                hidden[at] = term if step == 0 else hidden[at] + term
+            part = sum(jnp.sum(piece * piece, axis=1, keepdims=True) for piece in pieces)
+            sums = part if sums is None else sums + part
+        mlp_scale = lax.rsqrt(sums * (1.0 / width) + epsilon)
+        active = [jnp.maximum(units * mlp_scale, 0.0) for units in hidden]
+        squared = [(units * units).astype(bf16) for units in active]
+        squared_ref[...] = squared[0]
+        return squared
+
+    serves = (tp == 1) & (kv > 0)
 
     def down_copy(at, j, to_tp):
         return remote(down_send.at[at, to_tp], down_recv.at[2 * kv + tp], down_sem.at[0], down_sem.at[1], j, to_tp)
 
     def down_columns(first, columns):
         return jnp.dot(
-            squared, w_down_ref[:, pl.ds(pl.multiple_of(first, half), columns)], preferred_element_type=f32
+            squared_ref[...],
+            w_down_ref[:, pl.ds(pl.multiple_of(first, half), columns)],
+            preferred_element_type=f32,
         )
 
-    for at, j in enumerate(far):
-        if at == 0:
-            for i in range(2):
-                down_send[at, i] = down_columns((2 * j + i) * half, half).astype(bf16)
-                down_copy(at, j, i).start()
-        else:
-            term = down_columns(2 * j * half, 2 * half)
-            for i in range(2):
-                down_send[at, i] = term[:, i * half : (i + 1) * half].astype(bf16)
-                down_copy(at, j, i).start()
-    term = down_columns(2 * kv * half, 2 * half)
-    for i in range(2):
-        down_own[i] = term[:, i * half : (i + 1) * half]
-        down_send[n_kv - 1, i] = term[:, i * half : (i + 1) * half].astype(bf16)
-    down_copy(n_kv - 1, kv, other).start()
-    total = stream_all[kv, tp].astype(f32) + down_own[tp]
+    def down_chip(at, j):
+        term = down_columns(2 * j * half, 2 * half)
+        for i in range(2):
+            down_send[at, i] = term[:, i * half : (i + 1) * half].astype(bf16)
+            down_copy(at, j, i).start()
+
+    def down_pair():
+        term = down_columns(2 * kv * half, 2 * half)
+        for i in range(2):
+            down_own[i] = term[:, i * half : (i + 1) * half]
+            down_send[n_kv - 1, i] = term[:, i * half : (i + 1) * half].astype(bf16)
+        down_copy(n_kv - 1, kv, other).start()
+
+    @pl.when(serves)
+    def _():
+        waits = [[w_up_copy.wait_recv], [loads["down"].wait, w_down_copy.wait_recv]] + [[]] * (n_kv - 2)
+        squared = hidden_units((w_up_ref, w_up_other), waits)
+        for i in range(2):
+            cols = slice(i * half, (i + 1) * half)
+            term = jnp.dot(squared[0], w_down_ref[:, cols], preferred_element_type=f32)
+            term = term + jnp.dot(squared[1], w_down_other[:, cols], preferred_element_type=f32)
+            down_send[0, i] = term.astype(bf16)
+            down_copy(0, 0, i).start()
+
+    @pl.when(jnp.logical_not(serves))
+    def _():
+        hidden_units((w_up_ref,), [[], [loads["down"].wait]] + [[]] * (n_kv - 2))
+
+    @pl.when(kv == 0)
+    def _():
+        down_pair()
+        for j in range(n_kv - 1, 0, -1):
+            down_chip(j - 1, j)
+
+    @pl.when(kv > 0)
+    def _():
+        orders = [
+            sorted((j for j in range(1, n_kv) if j != me), key=lambda j: (-abs(j - me), j)) for me in range(n_kv)
+        ]
+        for at in range(n_kv - 2):
+            down_chip(at + 1, pick(kv, [order[at] for order in orders]))
+        down_pair()
+
 
     @pl.when(tp == 1)
     def _():
@@ -507,13 +564,32 @@
         some = stream_all.at[pl.ds(0, n_kv - 1)]
         remote(some, some, stream_send_sem.at[1], stream_recv_sem.at[0], kv, 0).wait_send()
 
-    some = down_recv.at[pl.ds(0, 2 * n_kv - 1)]
-    down_all = remote(some, some, down_sem.at[0], down_sem.at[1], kv, other)
-    down_all.wait_recv()
-    for slot in [2 * kv + other] + [2 * j + i for j in near for i in range(2)]:
-        total = total + down_recv[slot].astype(f32)
-    mixed_ref[...] = total.astype(bf16)
-    down_all.wait_send()
+    def down_blocks(count):
+        some = down_recv.at[pl.ds(0, count)]
+        return remote(some, some, down_sem.at[0], down_sem.at[1], kv, other)
+
+    def finish(count, slots):
+        total = stream_all[kv, tp].astype(f32) + down_own[tp]
+        down_blocks(count).wait_recv()
+        for slot in slots:
+            total = total + down_recv[slot].astype(f32)
+        mixed_ref[...] = total.astype(bf16)
+
+    @pl.when(kv == 0)
+    def _():
+        finish(n_kv, [other] + [2 * j + 1 for j in range(1, n_kv)])
+
+    @pl.when(kv > 0)
+    def _():
+        finish(2 * n_kv - 1, [2 * kv + other] + [2 * j + i for j in near for i in range(2)])
+
+    @pl.when((kv == 0) | (tp == 1))
+    def _():
+        down_blocks(2 * n_kv - 1).wait_send()
+
+    @pl.when((kv > 0) & (tp == 0))
+    def _():
+        down_blocks(2 * n_kv - 3).wait_send()
 
 
 def write_kernel(mixed_ref, state_ref, mixed_hbm, state_hbm, state_sem, mixed_sem):
@@ -570,6 +646,8 @@
         + [pltpu.VMEM(weight.shape, bf16) for weight in weights[3:]]
         + [
             pltpu.VMEM(w_out.shape, bf16),
+            pltpu.VMEM(w_up.shape, bf16),
+            pltpu.VMEM((w_down.shape[0], 2 * half), bf16),
             pltpu.VMEM((2, rows, half), bf16),
             pltpu.VMEM((n_kv, seqs, a_width), bf16),
             pltpu.VMEM((n_kv, seqs, val_width), bf16),
@@ -584,13 +662,14 @@
             pltpu.VMEM((2, n_kv, seqs, val_width), bf16),
             pltpu.VMEM((rows, val_width), f32),
             pltpu.VMEM((n_kv, 2, rows, half), bf16),
+            pltpu.VMEM((rows, w_up.shape[1]), bf16),
             pltpu.VMEM((n_kv, 2, rows, half), bf16),
             pltpu.VMEM((2, rows, half), f32),
             pltpu.VMEM((2 * n_kv, rows, half), bf16),
             dma((12,)),
             pltpu.SemaphoreType.REGULAR,
             dma((2,)),
-            dma,
+            dma((3,)),
             dma((3, 2)),
             dma((3,)),
             dma((2,)),

time: 24.1 us -> 23.3 us (0.967)
  Pallas kernels: 23.3 us -> 22.4 us
    pallas_call x1, Pallas kernels: 21.2 us -> 20.4 us  [kernel_shards(): pl.pallas_call(functools.partial(layer_kernel, n_kv), out_shape=(pltpu.VM...]
where the time goes in v3:
time: 23.3 us; the launch traced here: 23.1 us
  Pallas kernels  22.4 us (96%)
  between operations  0.64 us (3%)
    pallas_call x1, Pallas kernels, kernel_shards(): pl.pallas_call(functools.partial(layer_kernel, n_kv), out_shape=(pltpu.VM...  20.4 us
    pallas_call x1, Pallas kernels, kernel_shards(): pl.pallas_call(write_kernel, out_shape=(jax.ShapeDtypeStruct(tokens.shape...  2.08 us

profile of v3, /device:TPU:0, one launch (start us, length us, event | category | flops | bytes accessed | tf_op | source)
XLA Modules:
  0.0 23.1 jit_solution(1348718751219071634)
XLA Ops:
  0.6 20.4 %shard_map.149 = (bf16[16,256]{1,0:T(8,128)(2,1)S(1)}, f32[4,2,256,512]{3,2,1,0:T(8,128)S(1)}) custom-call(bf16[16,256]{1,0:T(8,128)(2,1)} %tok_hbm.1, f32[2,1,256]{2,1,0:T(1,128)} %bitcast.5, f32[1,512]{1,0:T(1,128)} %bitcast.6, f32[1,512]{1,0:T(1,128)} %bitcast.7, f32[4,2,1,256]{3,2,1,0:T(1,128)} %bitcast.4, f32[4,2,256,512]{3,2,1,0:T(8,128)} %state_hbm.1, ...), custom_call_target="tpu_custom_call" | custom-call | tf_op jit(solution)/shard_map/pallas_call | solution.py:680
  21.0 2.1 %shard_map.150 = (bf16[16,256]{1,0:T(8,128)(2,1)}, f32[4,2,256,512]{3,2,1,0:T(8,128)}) custom-call(bf16[16,256]{1,0:T(8,128)(2,1)S(1)} %get-tuple-element.4.mixed_ref, f32[4,2,256,512]{3,2,1,0:T(8,128)S(1)} %get-tuple-element.5.state_ref), custom_call_target="tpu_custom_call" | custom-call | tf_op jit(solution)/shard_map/pallas_call | solution.py:701

commit v4 on v3

--- a/solution.py
+++ b/solution.py
@@ -146,6 +146,8 @@
     w_out_ref,
     w_up_ref,
     w_down_ref,
+    w_qkd_other,
+    send_other,
     w_out_other,
     w_up_other,
     w_down_other,
@@ -209,10 +211,6 @@
     for j in far:
         signal(barrier, j, 1)
 
-        @pl.when(j > kv)
-        def _():
-            signal(barrier, j, 0)
-
     loads = {}
     at_sem = {}
     for name, source, target in (
@@ -240,7 +238,7 @@
 
     @pl.when(tp == 0)
     def _():
-        pl.semaphore_wait(barrier, 1 + 2 * kv)
+        pl.semaphore_wait(barrier, 1)
         signal(ready_sem, kv, 1)
 
     @pl.when(tp == 1)
@@ -258,6 +256,20 @@
         w_down_hbm.at[:, pl.ds(0, 2 * half)], w_down_other, w_out_sem.at[2], w_out_sem.at[2], kv, 1
     )
 
+    qkd_copies = [
+        remote(source, w_qkd_other.at[i], w_out_sem.at[1], w_out_sem.at[1], kv, 1)
+        for i, source in enumerate((wq_hbm, wk_hbm, wd_hbm))
+    ]
+    qkd_all = remote(w_qkd_other, w_qkd_other, w_out_sem.at[1], w_out_sem.at[1], kv, 1)
+    upper = kv * 2 >= n_kv
+    takes_over = (tp == 1) & (kv == 0)
+    hands_over = (tp == 0) & (kv == 0)
+
+    @pl.when(hands_over)
+    def _():
+        for copy in qkd_copies:
+            copy.start()
+
     @pl.when(tp == 0)
     def _():
         w_out_copy.start()
@@ -265,6 +277,15 @@
     @pl.when((tp == 0) & (kv > 0))
     def _():
         w_up_copy.start()
+
+
+    def group_is_here():
+        pl.semaphore_wait(barrier, 2 * (n_kv - 1))
+        signal(ready_sem, kv, 0)
+
+    @pl.when((tp == 1) & upper)
+    def _():
+        group_is_here()
 
     tok_all[tp] = tok_ref[...]
     tok_own = tok_ref[...].astype(f32)
@@ -305,21 +326,24 @@
         some = pl.ds(0, n_kv - 1)
         return remote(send.at[some], recv.at[some], proj_sem.at[group, 0], proj_sem.at[group, 1], kv, other)
 
-    def send_lower(group):
+    def send_early(group):
         for j in far:
 
-            @pl.when(j < kv)
+            @pl.when(upper & (j != kv - 1))
             def _():
                 proj_copy(group, j).start()
 
-    def send_higher():
+    def send_late():
         order = sorted(
             ((group, at) for group in range(3) for at in range(n_kv - 1)),
             key=lambda item: item[1] * 2 + (0 if item[0] == 0 else 3),
         )
         for group, at in order:
-
-            @pl.when(far[at] > kv)
+            sends = jnp.logical_not(upper)
+            if group == 0:
+                sends = sends & jnp.logical_not(hands_over)
+
+            @pl.when(sends)
             def _():
                 proj_copy(group, far[at]).start()
 
@@ -335,23 +359,54 @@
     ]
     for i in range(3):
         fill(send_a, early[i] + late[i], i * key_width)
-    send_lower(0)
+
+    @pl.when((tp == 0) & upper)
+    def _():
+        pl.semaphore_wait(ready_sem, 1)
+
+    send_early(0)
     project("v", wv_ref, send_b)
-    send_lower(1)
-
-    @pl.when(tp == 1)
-    def _():
-        pl.semaphore_wait(barrier, 2 * (n_kv - 1))
-        signal(ready_sem, kv, 0)
+    send_early(1)
+
+    def other_copy(j):
+        return remote(send_other.at[j], recv_a.at[0], w_out_sem.at[2], proj_sem.at[0, 1], j, 0)
+
+    @pl.when(takes_over)
+    def _():
+        qkd_all.wait_recv()
+        for owner in range(n_kv):
+            send_other[owner, :, 3 * key_width :] = send_a[owner, :, 3 * key_width :]
+        total = [
+            jnp.dot(scaled_own, w_qkd_other[i, half_rows(tp), :], preferred_element_type=f32)
+            + jnp.dot(scaled_other, w_qkd_other[i, half_rows(other), :], preferred_element_type=f32)
+            for i in range(3)
+        ]
+        for i in range(3):
+            fill(send_other, total[i], i * key_width)
+
+    @pl.when((tp == 1) & jnp.logical_not(upper))
+    def _():
+        group_is_here()
+
+    @pl.when(takes_over)
+    def _():
+        for j in range(n_kv - 1, 0, -1):
+            other_copy(j).start()
 
     project("g", wg_ref, send_c)
-    send_lower(2)
-
-    @pl.when(tp == 0)
+    send_early(2)
+
+    @pl.when(upper)
+    def _():
+        for group in range(3):
+            proj_copy(group, kv - 1).start()
+
+
+    @pl.when((tp == 0) & jnp.logical_not(upper))
     def _():
         pl.semaphore_wait(ready_sem, 1)
 
-    send_higher()
+    send_late()
 
     def gathered(group):
         send, recv = groups[group]
@@ -434,8 +489,22 @@
                 )
 
     tok_copy.wait_send()
-    for group in range(3):
+
+    @pl.when(jnp.logical_not(hands_over))
+    def _():
+        proj_all(0).wait_send()
+
+    for group in (1, 2):
         proj_all(group).wait_send()
+
+    @pl.when(takes_over)
+    def _():
+        some = send_other.at[pl.ds(0, n_kv - 1)]
+        remote(some, some, w_out_sem.at[2], w_out_sem.at[2], kv, 0).wait_send()
+
+    @pl.when(hands_over)
+    def _():
+        qkd_all.wait_send()
 
     def stream_copy(j, to_tp, owner):
         block = stream_all.at[owner]
@@ -645,6 +714,8 @@
         + [pltpu.VMEM((3,) + w_query.shape, bf16)]
         + [pltpu.VMEM(weight.shape, bf16) for weight in weights[3:]]
         + [
+            pltpu.VMEM((3,) + w_query.shape, bf16),
+            pltpu.VMEM((n_kv, seqs, a_width), bf16),
             pltpu.VMEM(w_out.shape, bf16),
             pltpu.VMEM(w_up.shape, bf16),
             pltpu.VMEM((w_down.shape[0], 2 * half), bf16),

time: 23.3 us -> 23.1 us (level)
  no operation moved by 1% of the time
where the time goes in v4:
time: 23.1 us; the launch traced here: 22.9 us
  Pallas kernels  22.3 us (97%)
  between operations  0.64 us (3%)
    pallas_call x1, Pallas kernels, kernel_shards(): pl.pallas_call(functools.partial(layer_kernel, n_kv), out_shape=(pltpu.VM...  20.2 us
    pallas_call x1, Pallas kernels, kernel_shards(): pl.pallas_call(write_kernel, out_shape=(jax.ShapeDtypeStruct(tokens.shape...  2.08 us

profile of v4, /device:TPU:0, one launch (start us, length us, event | category | flops | bytes accessed | tf_op | source)
XLA Modules:
  0.0 22.9 jit_solution(1745549208823821724)
XLA Ops:
  0.6 20.2 %shard_map.149 = (bf16[16,256]{1,0:T(8,128)(2,1)S(1)}, f32[4,2,256,512]{3,2,1,0:T(8,128)S(1)}) custom-call(bf16[16,256]{1,0:T(8,128)(2,1)} %tok_hbm.1, f32[2,1,256]{2,1,0:T(1,128)} %bitcast.5, f32[1,512]{1,0:T(1,128)} %bitcast.6, f32[1,512]{1,0:T(1,128)} %bitcast.7, f32[4,2,1,256]{3,2,1,0:T(1,128)} %bitcast.4, f32[4,2,256,512]{3,2,1,0:T(8,128)} %state_hbm.1, ...), custom_call_target="tpu_custom_call" | custom-call | tf_op jit(solution)/shard_map/pallas_call | solution.py:751
  20.8 2.1 %shard_map.150 = (bf16[16,256]{1,0:T(8,128)(2,1)}, f32[4,2,256,512]{3,2,1,0:T(8,128)}) custom-call(bf16[16,256]{1,0:T(8,128)(2,1)S(1)} %get-tuple-element.4.mixed_ref, f32[4,2,256,512]{3,2,1,0:T(8,128)S(1)} %get-tuple-element.5.state_ref), custom_call_target="tpu_custom_call" | custom-call | tf_op jit(solution)/shard_map/pallas_call | solution.py:772

commit v5 on v4

--- a/solution.py
+++ b/solution.py
@@ -159,6 +159,8 @@
     recv_b,
     recv_c,
     coef,
+    queries_t,
+    update,
     coef_t,
     vals,
     read,
@@ -312,10 +314,9 @@
         for owner in range(n_kv):
             send[owner, :, at : at + columns] = total[owner * seqs : (owner + 1) * seqs].astype(bf16)
 
-    def project(name, weight_ref, send):
-        loads[name].wait()
+    def project(weight_ref):
         total = jnp.dot(scaled_own, weight_ref[half_rows(tp), :], preferred_element_type=f32)
-        fill(send, total + jnp.dot(scaled_other, weight_ref[half_rows(other), :], preferred_element_type=f32), 0)
+        return total + jnp.dot(scaled_other, weight_ref[half_rows(other), :], preferred_element_type=f32)
 
     def proj_copy(group, j):
         send, recv = groups[group]
@@ -365,8 +366,18 @@
         pl.semaphore_wait(ready_sem, 1)
 
     send_early(0)
-    project("v", wv_ref, send_b)
+    loads["v"].wait()
+    loads["g"].wait()
+    total_v, total_g = project(wv_ref), project(wg_ref)
+    fill(send_b, total_v, 0)
+    fill(send_c, total_g, 0)
     send_early(1)
+    send_early(2)
+
+    @pl.when(upper)
+    def _():
+        for group in range(3):
+            proj_copy(group, kv - 1).start()
 
     def other_copy(j):
         return remote(send_other.at[j], recv_a.at[0], w_out_sem.at[2], proj_sem.at[0, 1], j, 0)
@@ -393,14 +404,6 @@
         for j in range(n_kv - 1, 0, -1):
             other_copy(j).start()
 
-    project("g", wg_ref, send_c)
-    send_early(2)
-
-    @pl.when(upper)
-    def _():
-        for group in range(3):
-            proj_copy(group, kv - 1).start()
-
 
     @pl.when((tp == 0) & jnp.logical_not(upper))
     def _():
@@ -426,37 +429,38 @@
         group_a[:, 2 * key_width : 3 * key_width] * row_scale + decay_offset_ref[...]
     )
     query_retain = queries * retain
-    overlap = queries * new_keys
     for h in range(heads):
-        cols = slice(h * key_dim, (h + 1) * key_dim)
-        coef[(3 * h) * seqs : (3 * h + 1) * seqs, :] = query_retain[:, cols]
-        coef[(3 * h + 1) * seqs : (3 * h + 2) * seqs, :] = new_keys[:, cols]
-        coef[(3 * h + 2) * seqs : (3 * h + 3) * seqs, :] = retain[:, cols]
-    coef_t[...] = coef[...].T
+        coef[h * seqs : (h + 1) * seqs, :] = query_retain[:, h * key_dim : (h + 1) * key_dim]
+    queries_t[...] = coef[...].T
     loads["state"].wait()
     for h in range(heads):
         for b in range(seqs):
-            at = 3 * h * seqs + b
+            at = h * seqs + b
             total = jnp.zeros((8, val_dim), f32)
             for start in range(0, key_dim, ROW_CHUNK):
                 piece = slice(start, start + ROW_CHUNK)
-                product = coef_t[piece, at : at + 1] * state_ref[b, h, piece, :]
+                product = queries_t[piece, at : at + 1] * state_ref[b, h, piece, :]
                 total = total + jnp.sum(product.reshape(ROW_CHUNK // 8, 8, val_dim), axis=0)
             read[h, b : b + 1, :] = jnp.sum(total, axis=0, keepdims=True)
 
+    overlap = queries * new_keys
+    all_dots = [
+        jnp.sum(overlap[:, h * key_dim : (h + 1) * key_dim], axis=1, keepdims=True) for h in range(heads)
+    ]
     values = gathered(1) * row_scale
     vals[...] = values
-    gates = gathered(2) * row_scale
     loads["head_gain"].wait()
+    normal = []
     for h in range(heads):
         cols = slice(h * val_dim, (h + 1) * val_dim)
-        dots = jnp.sum(overlap[:, h * key_dim : (h + 1) * key_dim], axis=1, keepdims=True)
-        readout = read[h] + dots * values[:, cols]
+        readout = read[h] + all_dots[h] * values[:, cols]
         mean = jnp.mean(readout * readout, axis=1, keepdims=True)
+        normal.append(readout * lax.rsqrt(mean + epsilon) * head_gain_ref[...])
+    gates = gathered(2) * row_scale
+    for h in range(heads):
+        cols = slice(h * val_dim, (h + 1) * val_dim)
         gate = gates[:, cols]
-        gated_all[tp, kv, :, cols] = (
-            readout * lax.rsqrt(mean + epsilon) * head_gain_ref[...] * (gate * jax.nn.sigmoid(gate))
-        ).astype(bf16)
+        gated_all[tp, kv, :, cols] = (normal[h] * (gate * jax.nn.sigmoid(gate))).astype(bf16)
 
     def gated_copy(j):
         block = gated_all.at[tp, kv]
@@ -478,14 +482,19 @@
         w_down_copy.start()
 
     for h in range(heads):
+        cols = slice(h * key_dim, (h + 1) * key_dim)
+        update[2 * h * seqs : (2 * h + 1) * seqs, :] = new_keys[:, cols]
+        update[(2 * h + 1) * seqs : (2 * h + 2) * seqs, :] = retain[:, cols]
+    coef_t[...] = update[...].T
+    for h in range(heads):
         for b in range(seqs):
-            at = 3 * h * seqs + b
+            at = 2 * h * seqs + b
             value_row = vals[b : b + 1, h * val_dim : (h + 1) * val_dim]
             for start in range(0, key_dim, ROW_CHUNK):
                 piece = slice(start, start + ROW_CHUNK)
                 state_ref[b, h, piece, :] = (
-                    coef_t[piece, at + 2 * seqs : at + 2 * seqs + 1] * state_ref[b, h, piece, :]
-                    + coef_t[piece, at + seqs : at + seqs + 1] * value_row
+                    coef_t[piece, at + seqs : at + seqs + 1] * state_ref[b, h, piece, :]
+                    + coef_t[piece, at : at + 1] * value_row
                 )
 
     tok_copy.wait_send()
@@ -700,8 +709,6 @@
     hbm = pl.BlockSpec(memory_space=pltpu.HBM)
     weights = (w_query, w_key, w_decay, w_value, w_gate, w_out, w_up, w_down)
     a_width = 3 * key_width + 128
-    coef_rows = 3 * heads * seqs
-    coef_rows += -coef_rows % 8
     dma = pltpu.SemaphoreType.DMA
     scratch = (
         [
@@ -726,8 +733,10 @@
             pltpu.VMEM((n_kv, seqs, a_width), bf16),
             pltpu.VMEM((n_kv, seqs, val_width), bf16),
             pltpu.VMEM((n_kv, seqs, val_width), bf16),
-            pltpu.VMEM((coef_rows, key_dim), f32),
-            pltpu.VMEM((key_dim, coef_rows), f32),
+            pltpu.VMEM((heads * seqs, key_dim), f32),
+            pltpu.VMEM((key_dim, heads * seqs), f32),
+            pltpu.VMEM((2 * heads * seqs, key_dim), f32),
+            pltpu.VMEM((key_dim, 2 * heads * seqs), f32),
             pltpu.VMEM((seqs, val_width), f32),
             pltpu.VMEM((heads, seqs, val_dim), f32),
             pltpu.VMEM((2, n_kv, seqs, val_width), bf16),

time: 23.1 us -> 22.9 us (level)
  no operation moved by 1% of the time
where the time goes in v5:
time: 22.9 us; the launch traced here: 22.7 us
  Pallas kernels  22.1 us (97%)
  between operations  0.64 us (3%)
    pallas_call x1, Pallas kernels, kernel_shards(): pl.pallas_call(functools.partial(layer_kernel, n_kv), out_shape=(pltpu.VM...  20 us
    pallas_call x1, Pallas kernels, kernel_shards(): pl.pallas_call(write_kernel, out_shape=(jax.ShapeDtypeStruct(tokens.shape...  2.08 us

profile of v5, /device:TPU:0, one launch (start us, length us, event | category | flops | bytes accessed | tf_op | source)
XLA Modules:
  0.0 22.7 jit_solution(15046434969011206543)
XLA Ops:
  0.6 20.0 %shard_map.149 = (bf16[16,256]{1,0:T(8,128)(2,1)S(1)}, f32[4,2,256,512]{3,2,1,0:T(8,128)S(1)}) custom-call(bf16[16,256]{1,0:T(8,128)(2,1)} %tok_hbm.1, f32[2,1,256]{2,1,0:T(1,128)} %bitcast.5, f32[1,512]{1,0:T(1,128)} %bitcast.6, f32[1,512]{1,0:T(1,128)} %bitcast.7, f32[4,2,1,256]{3,2,1,0:T(1,128)} %bitcast.4, f32[4,2,256,512]{3,2,1,0:T(8,128)} %state_hbm.1, ...), custom_call_target="tpu_custom_call" | custom-call | tf_op jit(solution)/shard_map/pallas_call | solution.py:760
  20.6 2.1 %shard_map.150 = (bf16[16,256]{1,0:T(8,128)(2,1)}, f32[4,2,256,512]{3,2,1,0:T(8,128)}) custom-call(bf16[16,256]{1,0:T(8,128)(2,1)S(1)} %get-tuple-element.4.mixed_ref, f32[4,2,256,512]{3,2,1,0:T(8,128)S(1)} %get-tuple-element.5.state_ref), custom_call_target="tpu_custom_call" | custom-call | tf_op jit(solution)/shard_map/pallas_call | solution.py:781

commit v6 on v5

--- a/solution.py
+++ b/solution.py
@@ -330,7 +330,11 @@
     def send_early(group):
         for j in far:
 
-            @pl.when(upper & (j != kv - 1))
+            now = upper & (j != kv - 1)
+            if group > 0 and j is not far[0]:
+                now = now & (j > kv)
+
+            @pl.when(now)
             def _():
                 proj_copy(group, j).start()
 
@@ -373,6 +377,13 @@
     fill(send_c, total_g, 0)
     send_early(1)
     send_early(2)
+
+    for j in far[1:]:
+        for group in (1, 2):
+
+            @pl.when(upper & (j < kv - 1))
+            def _():
+                proj_copy(group, j).start()
 
     @pl.when(upper)
     def _():

time: 22.9 us -> 22.9 us (level)
  no operation moved by 1% of the time
where the time goes in v6:
time: 22.9 us; the launch traced here: 22.7 us
  Pallas kernels  22 us (96%)
  between operations  0.64 us (3%)
    pallas_call x1, Pallas kernels, kernel_shards(): pl.pallas_call(functools.partial(layer_kernel, n_kv), out_shape=(pltpu.VM...  20 us
    pallas_call x1, Pallas kernels, kernel_shards(): pl.pallas_call(write_kernel, out_shape=(jax.ShapeDtypeStruct(tokens.shape...  2.08 us

profile of v6, /device:TPU:0, one launch (start us, length us, event | category | flops | bytes accessed | tf_op | source)
XLA Modules:
  0.0 22.7 jit_solution(6104499510672436590)
XLA Ops:
  0.6 20.0 %shard_map.149 = (bf16[16,256]{1,0:T(8,128)(2,1)S(1)}, f32[4,2,256,512]{3,2,1,0:T(8,128)S(1)}) custom-call(bf16[16,256]{1,0:T(8,128)(2,1)} %tok_hbm.1, f32[2,1,256]{2,1,0:T(1,128)} %bitcast.5, f32[1,512]{1,0:T(1,128)} %bitcast.6, f32[1,512]{1,0:T(1,128)} %bitcast.7, f32[4,2,1,256]{3,2,1,0:T(1,128)} %bitcast.4, f32[4,2,256,512]{3,2,1,0:T(8,128)} %state_hbm.1, ...), custom_call_target="tpu_custom_call" | custom-call | tf_op jit(solution)/shard_map/pallas_call | solution.py:771
  20.6 2.1 %shard_map.150 = (bf16[16,256]{1,0:T(8,128)(2,1)}, f32[4,2,256,512]{3,2,1,0:T(8,128)}) custom-call(bf16[16,256]{1,0:T(8,128)(2,1)S(1)} %get-tuple-element.4.mixed_ref, f32[4,2,256,512]{3,2,1,0:T(8,128)S(1)} %get-tuple-element.5.state_ref), custom_call_target="tpu_custom_call" | custom-call | tf_op jit(solution)/shard_map/pallas_call | solution.py:792
